TPU v7x, 32 devices: a whole 2x2x4 slice. The times are simulated.
32 devices in a mesh: sp: 8 (over z, x), tp: 4 (over y, core).
Axes of the slice: x: 2, y: 2, z: 4, core: 2. Of those that a mesh axis runs over, the one named last changes fastest.
Arguments:
- inputs: bfloat16 [3072, 2048], P('sp', 'tp'), may hold values from -6 to 6
- norm_gain: float32 [2048], replicated, may hold values from 0.1 to 1.9
- query_weight: bfloat16 [2048, 1024], P(None, 'tp')
- key_weight: bfloat16 [2048, 1024], P(None, 'tp'), may hold values from -0.15625 to 0.15625
- value_weight: bfloat16 [2048, 1024], P(None, 'tp'), may hold values from -0.125 to 0.125
- memory_query_weight: bfloat16 [2048, 1024], P(None, 'tp'), may hold values from -0.125 to 0.125
- memory_key_weight: bfloat16 [2048, 1024], P(None, 'tp'), may hold values from -0.125 to 0.125
- memory_value_weight: bfloat16 [2048, 1024], P(None, 'tp'), may hold values from -0.125 to 0.125
- input_gate_weight: bfloat16 [2048, 16], P(None, 'tp')
- forget_gate_weight: bfloat16 [2048, 16], P(None, 'tp'), may hold values from -0.3125 to 0.3125
- forget_bias: float32 [16], P('tp'), may hold values from 3 to 13
- decay_shift: float32 [3072, 16], P('sp', 'tp'), may hold values from -2 to 0, as said below
- lambdas: float32 [16], P('tp'), may hold values from 0.3 to 0.8
- head_gain: float32 [64], replicated, may hold values from 0.1 to 1.9
- out_weight_attention: bfloat16 [1024, 2048], P('tp'), may hold values from -0.125 to 0.125
- out_weight_memory: bfloat16 [1024, 2048], P('tp'), may hold values from -0.125 to 0.125
Outputs:
- combined: bfloat16 [3072, 2048], P('sp', 'tp')
Inputs may be any that keep to these rules, and one draw needn't show every extreme that they name: `decay_shift`: never positive.
All inputs are finite; a program needn't handle non-finite values.
Results may differ from a plain program's by a relative error of at most 0.018.
The roundings to bfloat16 on the way count: a program that leaves them out, or rounds other values in their place, can miss the bound.
Values may be sent and summed in bfloat16 or wider, within the bound.
A program may use at most 192 MiB of HBM per device.

v0:
```python
import functools

import jax
import jax.numpy as jnp
from jax import lax
from jax.experimental import pallas as pl
from jax.experimental.pallas import tpu as pltpu
from jax.sharding import PartitionSpec as P

HEAD = 64
DD = 32
EPSILON = 1e-06
ROTARY_BASE = 10000.0
NEGATIVE = -1e30
LOG2E = 1.4426950408889634
CORES = 2
STATE_ROWS = HEAD + 8
VMEM = pl.BlockSpec(memory_space=pltpu.VMEM)
MESH = pl.DeviceIdType.MESH
VMEM_LIMIT = 60 * 1024 * 1024


def signal(semaphore, axis, place):
    pl.semaphore_signal(semaphore, inc=1, device_id={axis: place}, device_id_type=MESH)


def remote(source, target, send_sem, recv_sem, axis, place):
    return pltpu.make_async_remote_copy(
        src_ref=source,
        dst_ref=target,
        send_sem=send_sem,
        recv_sem=recv_sem,
        device_id={axis: place},
        device_id_type=MESH,
    )


def tp_barrier(me, row_places):
    core = lax.rem(me, CORES)
    line = me // CORES
    barrier = pltpu.get_barrier_semaphore()
    signal(barrier, "tp", line * CORES + (1 - core))
    for step in range(1, row_places):
        signal(barrier, "tp", lax.rem(line + step, row_places) * CORES + core)
    pl.semaphore_wait(barrier, row_places)


def gather_kernel(size, chunks, x_ref, out_ref, local_sem, send_sems, recv_sems, pair_send, pair_recv):
    rows, columns = x_ref.shape
    lines = size // CORES
    me = lax.axis_index("tp")
    core = lax.rem(me, CORES)
    line = me // CORES
    pair = line * CORES + (1 - core)
    tp_barrier(me, lines)
    span = rows // chunks

    def place(owner, chunk):
        return out_ref.at[
            pl.ds(chunk * span, span), pl.ds(pl.multiple_of(owner * columns, 128), columns)
        ]

    sends = []
    for chunk in range(chunks):
        for step in range(1, lines):
            other = lax.rem(line + step, lines) * CORES + core
            copy = remote(
                x_ref.at[pl.ds(chunk * span, span)],
                place(me, chunk),
                send_sems.at[step, chunk],
                recv_sems.at[step, chunk],
                "tp",
                other,
            )
            copy.start()
            sends.append(copy)
    own = pltpu.make_async_copy(
        x_ref, out_ref.at[:, pl.ds(pl.multiple_of(me * columns, 128), columns)], local_sem
    )
    own.start()
    pairs = []
    for chunk in range(chunks):
        copy = remote(
            x_ref.at[pl.ds(chunk * span, span)],
            place(me, chunk),
            pair_send.at[0, chunk],
            pair_recv.at[0, chunk],
            "tp",
            pair,
        )
        copy.start()
        pairs.append(copy)
    for chunk in range(chunks):
        for step in range(1, lines):
            source = lax.rem(line + lines - step, lines) * CORES + core
            arrived = remote(
                place(source, chunk),
                place(source, chunk),
                send_sems.at[step, chunk],
                recv_sems.at[step, chunk],
                "tp",
                pair,
            )
            arrived.wait_recv()
            copy = remote(
                place(source, chunk),
                place(source, chunk),
                pair_send.at[step, chunk],
                pair_recv.at[step, chunk],
                "tp",
                pair,
            )
            copy.start()
            pairs.append(copy)
    own.wait()
    for copy in sends:
        copy.wait_send()
    for copy in pairs:
        copy.wait()


def head_mask(width, head):
    lanes = lax.broadcasted_iota(jnp.int32, (1, width), 1)
    return (lanes // HEAD) == head


def spread(columns, width):
    spreaded = columns[:, 0:1]
    for head in range(1, columns.shape[1]):
        lanes = lax.broadcasted_iota(jnp.int32, (1, width), 1)
        spreaded = jnp.where(lanes >= head * HEAD, columns[:, head : head + 1], spreaded)
    return jnp.broadcast_to(spreaded, (columns.shape[0], width))


def two_parts(floats):
    high = floats.astype(jnp.bfloat16)
    return high, (floats - high.astype(jnp.float32)).astype(jnp.bfloat16)


def dot(a, b, dims=((1,), (0,))):
    return lax.dot_general(a, b, (dims, ((), ())), preferred_element_type=jnp.float32)


def project_kernel(
    size, chunks, shard_ref, gain_ref, cos_ref, sin_ref, wq, wk, wv, wmq, wmk, wmv, wi, wf, bias_ref, shift_ref,
    q_out, kv_out, mq_out, mk_out, mv_out, gate_out, gate_row_out, state_out,
    sq, sk, sv, smq, smk, smv, sems, x_ref, local_sem, send_sems, recv_sems, pair_send, pair_recv,
):
    copies = []
    for place, (source, target) in enumerate(
        ((wq, sq), (wk, sk), (wv, sv), (wmq, smq), (wmk, smk), (wmv, smv))
    ):
        copy = pltpu.make_async_copy(source, target, sems.at[place])
        copy.start()
        copies.append(copy)
    gather_kernel(
        size, chunks, shard_ref, x_ref, local_sem, send_sems, recv_sems, pair_send, pair_recv
    )
    rows, features = x_ref.shape
    width = q_out.shape[1]
    heads = width // HEAD
    floats = x_ref[...].astype(jnp.float32)
    inverse = lax.rsqrt(
        jnp.sum(floats * floats, axis=1, keepdims=True) / features + EPSILON
    )
    scaled = (floats * gain_ref[...]).astype(jnp.bfloat16)
    gate = dot(scaled, wi[...], ((1,), (1,))) * inverse
    pre = dot(scaled, wf[...], ((1,), (1,))) * inverse + bias_ref[...]
    shift = shift_ref[...]
    shift = jnp.concatenate(
        [shift, jnp.zeros((128 - shift.shape[0], rows), jnp.float32)], axis=0
    ).T[:, : shift.shape[0]]
    forget = jnp.minimum(pre, 0.0) - jnp.log1p(jnp.exp(-jnp.abs(pre))) + shift
    row_index = lax.broadcasted_iota(jnp.int32, (rows, rows), 0)
    column_index = lax.broadcasted_iota(jnp.int32, (rows, rows), 1)
    lower = (column_index <= row_index).astype(jnp.bfloat16)
    first, rest = two_parts(forget)
    second = (forget - first.astype(jnp.float32) - rest.astype(jnp.float32)).astype(jnp.bfloat16)
    cumulative = dot(lower, first) + (dot(lower, rest) + dot(lower, second))

    def product(place, scratch):
        copies[place].wait()
        return (dot(scaled, scratch[...]) * inverse).astype(jnp.bfloat16)

    groups = width // 128
    cosine = jnp.concatenate([cos_ref[...]] * (128 * 2 // DD), axis=0).T
    sine = jnp.concatenate([-sin_ref[...], sin_ref[...]] * (128 // DD), axis=0).T
    cosine = jnp.concatenate([cosine] * groups, axis=1)
    sine = jnp.concatenate([sine] * groups, axis=1)
    lanes = lax.broadcasted_iota(jnp.int32, (1, width), 1)
    former = lax.rem(lanes, DD) < DD // 2

    def rotated(values):
        wide = values.astype(jnp.float32)
        partner = jnp.where(
            former, pltpu.roll(wide, width - DD // 2, 1), pltpu.roll(wide, DD // 2, 1)
        )
        return (wide * cosine + partner * sine).astype(jnp.bfloat16)

    q_out[...] = rotated(product(0, sq))
    kv_out[:, :width] = rotated(product(1, sk))
    kv_out[:, width:] = product(2, sv)
    mq_out[...] = product(3, smq)
    memory_keys = product(4, smk)
    memory_values = product(5, smv)
    mk_out[...] = memory_keys
    mv_out[...] = memory_values

    end = cumulative[rows - 1 : rows, :]
    toward = end - cumulative + gate
    top = jnp.max(toward, axis=0, keepdims=True)
    weights = spread(jnp.exp(toward - top), width)
    keyed = memory_keys.astype(jnp.float32) * (HEAD**-0.5) * weights
    high, low = two_parts(keyed)
    whole = dot(high, memory_values, ((0,), (0,))) + dot(low, memory_values, ((0,), (0,)))
    memory = jnp.zeros((HEAD, width), jnp.float32)
    for head in range(heads):
        memory = jnp.where(
            head_mask(width, head), whole[head * HEAD : (head + 1) * HEAD, :], memory
        )
    state_out[:HEAD, :] = memory
    state_out[HEAD : HEAD + 1, :] = jnp.sum(keyed, axis=0, keepdims=True)
    state_out[HEAD + 1 : HEAD + 2, :] = spread(top, width)
    state_out[HEAD + 2 : HEAD + 3, :] = spread(end, width)
    state_out[HEAD + 3 :, :] = jnp.zeros((STATE_ROWS - HEAD - 3, width), jnp.float32)
    gate_out[...] = cumulative
    offsets = jnp.concatenate(
        [gate - cumulative, jnp.zeros((rows, 128 - heads), jnp.float32)], axis=1
    )
    gate_row_out[...] = offsets.T[:8, :]


def span_barrier(me, depth, across):
    z = me // across
    x = lax.rem(me, across)
    barrier = pltpu.get_barrier_semaphore()

    @pl.when(z > 0)
    def _():
        signal(barrier, "sp", me - across)

    @pl.when(z < depth - 1)
    def _():
        signal(barrier, "sp", me + across)

    for step in range(1, across):
        signal(barrier, "sp", z * across + lax.rem(x + step, across))
    beside = (z > 0).astype(jnp.int32) + (z < depth - 1).astype(jnp.int32)
    pl.semaphore_wait(barrier, across - 1 + beside)


def mixer_kernel(
    depth, across, q_ref, kv_ref, mq_ref, mk_ref, mv_ref, cumulative_ref, offset_ref, own_state_ref,
    lambda_ref, gain_ref, woa, wom, out_ref, attended_ref, memory_ref, soa, som,
    chosen_ref, top_ref, total_ref, sums_ref, kv_all, state_ref, sems,
    kv_send, kv_recv, st_send, st_recv,
):
    load_attention = pltpu.make_async_copy(woa, soa, sems.at[0])
    load_memory = pltpu.make_async_copy(wom, som, sems.at[1])
    load_attention.start()
    load_memory.start()
    me = lax.axis_index("sp")
    z = me // across
    x = lax.rem(me, across)
    span_barrier(me, depth, across)

    def transfers(back, target, slot, place, own):
        return [
            remote(
                mine if own else everything.at[slot],
                everything.at[slot],
                send.at[back, target],
                recv.at[slot],
                "sp",
                place,
            )
            for mine, everything, send, recv in (
                (own_state_ref, state_ref, st_send, st_recv),
                (kv_ref, kv_all, kv_send, kv_recv),
            )
        ]

    def arrived(slot):
        for copy in transfers(0, 0, slot, me, False):
            copy.wait_recv()

    def onward(back, act, own=False):
        slot = me - back * across
        for step in range(1, across):
            other = lax.rem(x + step, across)

            def sideways():
                for copy in transfers(back, step, slot, z * across + other, own):
                    act(copy)

            if own:
                pl.when(x < other)(sideways)
            else:
                sideways()

        @pl.when(z < depth - 1)
        def _():
            for copy in transfers(back, 0, slot, me + across, own):
                act(copy)

    onward(0, lambda copy: copy.start(), True)
    rows, width = q_ref.shape
    heads = width // HEAD
    row_index = lax.broadcasted_iota(jnp.int32, (rows, rows), 0)
    column_index = lax.broadcasted_iota(jnp.int32, (rows, rows), 1)
    lower = column_index <= row_index
    factor = (DD**-0.5) * LOG2E
    lanes = lax.broadcasted_iota(jnp.int32, (1, 128), 1)

    upper = row_index <= column_index
    for head in range(heads):
        group = slice(head // 2 * 128, head // 2 * 128 + 128)
        for half in range(2):
            chosen = (lanes // DD) == (head % 2) * 2 + half
            chosen_ref[head * 2 + half] = jnp.where(chosen, q_ref[:, group], 0)

    def block(source, diagonal):
        for head in range(heads):
            group = slice(head // 2 * 128, head // 2 * 128 + 128)
            value_group = slice(width + head // 2 * 128, width + head // 2 * 128 + 128)
            if head % 2 == 0:
                turned = source[:, value_group].T
            values = turned[(head % 2) * HEAD : (head % 2 + 1) * HEAD, :]
            for half in range(2):
                index = head * 2 + half
                at = slice(index, index + 1)
                rows_at = slice(index * HEAD, (index + 1) * HEAD)
                scores = dot(source[:, group], chosen_ref[index], ((1,), (1,)))
                if diagonal:
                    scores = jnp.where(upper, scores, NEGATIVE)
                top = jnp.max(scores, axis=0, keepdims=True)
                if not diagonal:
                    old_top = top_ref[at, :]
                    top = jnp.maximum(top, old_top)
                weights = jnp.exp2((scores - top) * factor)
                total = jnp.sum(weights, axis=0, keepdims=True)
                sums = dot(values, weights.astype(jnp.bfloat16))
                if not diagonal:
                    shrink = jnp.exp2((old_top - top) * factor)
                    total = total + total_ref[at, :] * shrink
                    sums = sums + sums_ref[rows_at, :] * shrink
                top_ref[at, :] = top
                total_ref[at, :] = total
                sums_ref[rows_at, :] = sums

    block(kv_ref, True)

    def beside(back):
        def one(step, unused):
            other = lax.rem(x + step, across)

            @pl.when((back > 0) | (other < x))
            def _():
                slot = (z - back) * across + other
                arrived(slot)
                block(kv_all.at[slot], False)

            return unused

        lax.fori_loop(1, across, one, 0)

    def earlier(back, unused):
        slot = me - back * across
        arrived(slot)
        onward(back, lambda copy: copy.start())
        beside(back - 1)
        block(kv_all.at[slot], False)
        return unused

    lax.fori_loop(1, z + 1, earlier, 0)
    beside(z)
    state = jnp.zeros((STATE_ROWS, width), jnp.float32)

    def advance(place, carried):
        body, stable = carried
        later = state_ref[place]
        later_top = later[HEAD + 1 : HEAD + 2, :]
        decay = later[HEAD + 2 : HEAD + 3, :]
        new = jnp.maximum(decay + stable, later_top)
        return jnp.exp(decay + stable - new) * body + jnp.exp(later_top - new) * later, new

    state, stable = lax.fori_loop(0, me, advance, (state, jnp.zeros((1, width), jnp.float32)))
    memory_in = state[:HEAD, :]
    normal_in = state[HEAD : HEAD + 1, :]
    blocks = jnp.concatenate(
        [jnp.where(head_mask(width, head), memory_in, 0.0) for head in range(heads)], axis=0
    )
    high, low = two_parts(blocks)
    memory_queries = mq_ref[...]
    carried_part = dot(memory_queries, high) + dot(memory_queries, low)
    weighted = memory_queries.astype(jnp.float32) * normal_in
    for group in range(width // 128):
        span = slice(group * 128, (group + 1) * 128)
        keys = mk_ref[:, span]
        values = mv_ref[:, span]
        group_queries = mq_ref[:, span]
        result = None
        for side in range(2):
            head = group * 2 + side
            chosen = (lanes // HEAD) == side
            column = cumulative_ref[:, head : head + 1]
            gaps = jnp.where(lower, column + offset_ref[head : head + 1, :], NEGATIVE)
            carried_log = column + stable[:, head * HEAD : head * HEAD + 1]
            row_top = jnp.maximum(carried_log, jnp.max(gaps, axis=1, keepdims=True))
            within = jnp.exp(gaps - row_top)
            outside = jnp.exp(carried_log - row_top)
            scores = dot(jnp.where(chosen, group_queries, 0), keys, ((1,), (1,)))
            scores = jnp.where(lower, within * (scores * (HEAD**-0.5)), 0.0)
            denominator = jnp.sum(scores, axis=1, keepdims=True) + outside * jnp.sum(
                jnp.where(chosen, weighted[:, span], 0.0), axis=1, keepdims=True
            )
            score_high, score_low = two_parts(scores)
            numerator = dot(score_high, values) + dot(score_low, values)
            numerator = numerator + outside * carried_part[:, span]
            quotient = numerator / jnp.maximum(jnp.abs(denominator), 1.0)
            result = quotient if result is None else jnp.where(chosen, quotient, result)
        memory_ref[:, span] = result.astype(jnp.bfloat16)

    eye = lax.broadcasted_iota(jnp.int32, (HEAD, HEAD), 0) == lax.broadcasted_iota(
        jnp.int32, (HEAD, HEAD), 1
    )
    gain = jnp.sum(jnp.where(eye, gain_ref[...], 0.0), axis=1, keepdims=True)
    for head in range(heads):
        first, second = (
            sums_ref[index * HEAD : (index + 1) * HEAD, :] / total_ref[index : index + 1, :]
            for index in (head * 2, head * 2 + 1)
        )
        difference = first - lambda_ref[:, head : head + 1] * second
        mean = jnp.mean(difference * difference, axis=0, keepdims=True)
        attended_ref[head * HEAD : (head + 1) * HEAD, :] = (
            difference * lax.rsqrt(mean + EPSILON) * gain
        ).astype(jnp.bfloat16)
    onward(0, lambda copy: copy.wait_send(), True)

    def finish(back, unused):
        onward(back, lambda copy: copy.wait_send())
        return unused

    lax.fori_loop(1, z + 1, finish, 0)
    load_attention.wait()
    load_memory.wait()
    out_ref[...] = (
        dot(attended_ref[...], soa[...], ((0,), (0,))) + dot(memory_ref[...], som[...])
    ).astype(jnp.bfloat16)


def scatter_kernel(size, chunks, part_ref, out_ref, pair_in, line_out, line_in, pair_send, pair_recv, line_send, line_recv):
    rows, columns = out_ref.shape
    lines = size // CORES
    me = lax.axis_index("tp")
    core = lax.rem(me, CORES)
    line = me // CORES
    pair = line * CORES + (1 - core)
    tp_barrier(me, lines)
    span = rows // chunks

    def columns_of(owner):
        return pl.ds(pl.multiple_of(owner * columns, 128), columns)

    def rows_of(chunk):
        return pl.ds(chunk * span, span)

    order = list(range(1, lines)) + [0]
    pairs = {}
    for chunk in range(chunks):
        for step in order:
            target = lax.rem(line + step, lines) * CORES + (1 - core)
            copy = remote(
                part_ref.at[rows_of(chunk), columns_of(target)],
                pair_in.at[step, rows_of(chunk)],
                pair_send.at[step, chunk],
                pair_recv.at[step, chunk],
                "tp",
                pair,
            )
            copy.start()
            pairs[step, chunk] = copy

    def pair_sum(step, chunk):
        pairs[step, chunk].wait_recv()
        mine = part_ref[rows_of(chunk), columns_of(lax.rem(line + step, lines) * CORES + core)]
        return mine.astype(jnp.float32) + pair_in[step, rows_of(chunk), :].astype(jnp.float32)

    sends = {}
    for chunk in range(chunks):
        for step in range(1, lines):
            line_out[step, rows_of(chunk), :] = pair_sum(step, chunk).astype(jnp.bfloat16)
            copy = remote(
                line_out.at[step, rows_of(chunk)],
                line_in.at[step, rows_of(chunk)],
                line_send.at[step, chunk],
                line_recv.at[step, chunk],
                "tp",
                lax.rem(line + step, lines) * CORES + core,
            )
            copy.start()
            sends[step, chunk] = copy
    for chunk in range(chunks):
        total = pair_sum(0, chunk)
        for step in range(1, lines):
            sends[step, chunk].wait_recv()
            total = total + line_in[step, rows_of(chunk), :].astype(jnp.float32)
        out_ref[rows_of(chunk), :] = total.astype(jnp.bfloat16)
    for copy in pairs.values():
        copy.wait_send()
    for copy in sends.values():
        copy.wait_send()


def per_device(tp_size, depth, across, inputs, norm_gain, query_weight, key_weight, value_weight,
               memory_query_weight, memory_key_weight, memory_value_weight, input_gate_weight,
               forget_gate_weight, forget_bias, decay_shift, lambdas, head_gain,
               out_weight_attention, out_weight_memory):
    rows, columns = inputs.shape
    features = norm_gain.shape[0]
    width = query_weight.shape[1]
    heads = width // HEAD
    lines = tp_size // CORES
    spans = depth * across
    chunks = 4
    dma = pltpu.SemaphoreType.DMA

    def params(**more):
        return pltpu.CompilerParams(vmem_limit_bytes=VMEM_LIMIT, **more)

    middle = DD // 2
    inverse = 1.0 / ROTARY_BASE ** (jnp.arange(middle, dtype=jnp.float32) / middle)
    positions = lax.axis_index("sp") * rows + jnp.arange(rows, dtype=jnp.int32)
    angles = inverse[:, None] * positions.astype(jnp.float32)[None, :]
    cosine = jnp.cos(angles)
    sine = jnp.sin(angles)

    hbm = pl.BlockSpec(memory_space=pl.ANY)
    half = jax.ShapeDtypeStruct((rows, width), jnp.bfloat16)
    queries, packed, memory_queries, memory_keys, memory_values, cumulative, offsets, state = pl.pallas_call(
        functools.partial(project_kernel, tp_size, chunks),
        out_shape=[
            half,
            jax.ShapeDtypeStruct((rows, 2 * width), jnp.bfloat16),
            half,
            half,
            half,
            jax.ShapeDtypeStruct((rows, heads), jnp.float32),
            jax.ShapeDtypeStruct((8, rows), jnp.float32),
            jax.ShapeDtypeStruct((STATE_ROWS, width), jnp.float32),
        ],
        in_specs=[VMEM] * 4 + [hbm] * 6 + [VMEM] * 4,
        out_specs=[VMEM] * 8,
        scratch_shapes=[pltpu.VMEM((features, width), jnp.bfloat16)] * 6
        + [dma((6,)), pltpu.VMEM((rows, features), jnp.bfloat16), dma(())]
        + [dma((lines, chunks))] * 4,
        compiler_params=params(collective_id=0, has_side_effects=True),
        name="project",
    )(
        inputs, norm_gain[None, :], cosine, sine, query_weight, key_weight, value_weight,
        memory_query_weight, memory_key_weight, memory_value_weight, input_gate_weight.T,
        forget_gate_weight.T, forget_bias[None, :], decay_shift.T,
    )

    partial_term = pl.pallas_call(
        functools.partial(mixer_kernel, depth, across),
        out_shape=jax.ShapeDtypeStruct((rows, features), jnp.bfloat16),
        in_specs=[VMEM] * 10 + [hbm] * 2,
        out_specs=VMEM,
        scratch_shapes=[
            pltpu.VMEM((width, rows), jnp.bfloat16),
            pltpu.VMEM((rows, width), jnp.bfloat16),
            pltpu.VMEM((width, features), jnp.bfloat16),
            pltpu.VMEM((width, features), jnp.bfloat16),
            pltpu.VMEM((2 * heads, rows, 128), jnp.bfloat16),
            pltpu.VMEM((2 * heads, rows), jnp.float32),
            pltpu.VMEM((2 * heads, rows), jnp.float32),
            pltpu.VMEM((2 * width, rows), jnp.float32),
            pltpu.VMEM((spans, rows, 2 * width), jnp.bfloat16),
            pltpu.VMEM((spans, STATE_ROWS, width), jnp.float32),
            dma((2,)), dma((depth, across)), dma((spans,)), dma((depth, across)), dma((spans,)),
        ],
        compiler_params=params(collective_id=1, has_side_effects=True),
        name="mixers",
    )(
        queries, packed, memory_queries, memory_keys, memory_values, cumulative, offsets,
        state, lambdas[None, :], head_gain[None, :], out_weight_attention,
        out_weight_memory,
    )

    return pl.pallas_call(
        functools.partial(scatter_kernel, tp_size, chunks),
        out_shape=jax.ShapeDtypeStruct((rows, columns), jnp.bfloat16),
        in_specs=[VMEM],
        out_specs=VMEM,
        scratch_shapes=[
            pltpu.VMEM((lines, rows, columns), jnp.bfloat16),
            pltpu.VMEM((lines, rows, columns), jnp.bfloat16),
            pltpu.VMEM((lines, rows, columns), jnp.bfloat16),
            dma((lines, chunks)), dma((lines, chunks)), dma((lines, chunks)), dma((lines, chunks)),
        ],
        compiler_params=params(collective_id=2, has_side_effects=True),
        name="scatter_output",
    )(partial_term)


def columns_across(mesh):
    spans = mesh.shape["sp"]
    try:
        places = {device.coords[0] for device in mesh.devices.flat}
        across = len(places)
    except AttributeError:
        across = 2
    return across if spans % across == 0 else 1


def solution(mesh):
    across = columns_across(mesh)
    in_specs = (
        P("sp", "tp"),
        P(),
        P(None, "tp"),
        P(None, "tp"),
        P(None, "tp"),
        P(None, "tp"),
        P(None, "tp"),
        P(None, "tp"),
        P(None, "tp"),
        P(None, "tp"),
        P("tp"),
        P("sp", "tp"),
        P("tp"),
        P(),
        P("tp", None),
        P("tp", None),
    )
    return jax.shard_map(
        functools.partial(
            per_device, mesh.shape["tp"], mesh.shape["sp"] // across, across
        ),
        mesh=mesh,
        in_specs=in_specs,
        out_specs=P("sp", "tp"),
        check_vma=False,
    )
```

profile of v0, /device:TPU:25, one launch (start us, length us, event | category | flops | bytes accessed | tf_op | source)
XLA Modules:
  0.0 94.4 jit_solution(16694483370052124090)
XLA Ops:
  0.0 0.8 multiply_sine_fusion
  0.8 22.7 %project.1 = (bf16[384,256]{1,0:T(8,128)(2,1)}, bf16[384,512]{1,0:T(8,128)(2,1)}, bf16[384,256]{1,0:T(8,128)(2,1)}, bf16[384,256]{1,0:T(8,128)(2,1)}, bf16[384,2...) custom-call(bf16[384,512]{1,0:T(8,128)(2,1)} %shard_ref.1, f32[1,2048]{1,0:T(1,128)} %bitcast.9, ...), custom_call_target="tpu_custom_call" | custom-call | tf_op jit(solution)/shard_map/project/pallas_call | solution.py:540
  23.5 52.5 %mixers.1.part_ref = bf16[384,2048]{1,0:T(8,128)(2,1)} custom-call(bf16[384,256]{1,0:T(8,128)(2,1)} %get-tuple-element.13.q_ref, bf16[384,512]{1,0:T(8,128)(2,1)} %get-tuple-element.14.kv_ref, bf16[384,256]{1,0:T(8,128)(2,1)} %get-tuple-element.15.mq_ref, bf16[384,256]{1,0:T(8,128)(2,1)} %get-tuple-element.16.mk_ref, ...), custom_call_target="tpu_custom_call" | custom-call | tf_op jit(solution)/shard_map/mixers/pallas_call | solution.py:565
  76.1 16.6 %scatter_output.1 = bf16[384,512]{1,0:T(8,128)(2,1)} custom-call(bf16[384,2048]{1,0:T(8,128)(2,1)} %mixers.1.part_ref), custom_call_target="tpu_custom_call" | custom-call | tf_op jit(solution)/shard_map/scatter_output/pallas_call | solution.py:591
  92.6 1.8 %copy.18 = bf16[384,512]{1,0:T(8,128)(2,1)} copy(bf16[384,512]{1,0:T(8,128)(2,1)} %scatter_output.1) | data formatting | bytes 786432
  (2 shorter events, 0.0 us)
where the time goes:
time: 94.6 us; the launch traced here: 94.4 us
  Pallas kernels  91.8 us (97%)
  local copies, waits for them, and re-layouts  1.77 us (2%)
    pallas_call x1, Pallas kernels, per_device(): pl.pallas_call(functools.partial(mixer_kernel, depth, across), out_shape=...  52.5 us
    pallas_call x1, Pallas kernels, per_device(): pl.pallas_call(functools.partial(project_kernel, tp_size, chunks), out_sh...  22.7 us
    pallas_call x1, Pallas kernels, per_device(): pl.pallas_call(functools.partial(scatter_kernel, tp_size, chunks), out_sh...  16.6 us

commit v1 on v0

v1 whole, which is shorter than its diff:
```python
import functools

import jax
import jax.numpy as jnp
from jax import lax
from jax.experimental import pallas as pl
from jax.experimental.pallas import tpu as pltpu
from jax.sharding import PartitionSpec as P

HEAD = 64
DD = 32
EPSILON = 1e-06
ROTARY_BASE = 10000.0
NEGATIVE = -1e30
LOG2E = 1.4426950408889634
CORES = 2
STATE_ROWS = HEAD + 8
VALUE_ROWS = HEAD + 16
VMEM = pl.BlockSpec(memory_space=pltpu.VMEM)
MESH = pl.DeviceIdType.MESH
VMEM_LIMIT = 60 * 1024 * 1024
TILE = 256


def signal(semaphore, axis, place):
    pl.semaphore_signal(semaphore, inc=1, device_id={axis: place}, device_id_type=MESH)


def remote(source, target, send_sem, recv_sem, axis, place):
    return pltpu.make_async_remote_copy(
        src_ref=source,
        dst_ref=target,
        send_sem=send_sem,
        recv_sem=recv_sem,
        device_id={axis: place},
        device_id_type=MESH,
    )


def head_mask(width, head):
    lanes = lax.broadcasted_iota(jnp.int32, (1, width), 1)
    return (lanes // HEAD) == head


def spread(columns, width):
    spreaded = columns[:, 0:1]
    for head in range(1, columns.shape[1]):
        lanes = lax.broadcasted_iota(jnp.int32, (1, width), 1)
        spreaded = jnp.where(lanes >= head * HEAD, columns[:, head : head + 1], spreaded)
    return jnp.broadcast_to(spreaded, (columns.shape[0], width))


def two_parts(floats):
    high = floats.astype(jnp.bfloat16)
    return high, (floats - high.astype(jnp.float32)).astype(jnp.bfloat16)


def dot(a, b, dims=((1,), (0,))):
    return lax.dot_general(a, b, (dims, ((), ())), preferred_element_type=jnp.float32)


def near_first(place, count, rank):
    both = jnp.minimum(place, count - 1 - place)
    half = (rank + 1) // 2
    alternating = jnp.where(rank % 2 == 1, place - half, place + half)
    one_sided = jnp.where(place < count - 1 - place, rank, count - 1 - rank)
    return jnp.where(rank <= 2 * both, alternating, one_sided)


def layer_kernel(
    size, depth, across, chunks, out_chunks,
    shard_ref, gain_ref, cos_ref, sin_ref, wq, wk, wv, wmq, wmk, wmv, wi, wf, bias_ref, shift_ref,
    lambda_ref, head_gain_ref, woa, wom,
    out_ref,
    sq, sk, sv, smq, smk, smv, soa, som, x_ref, scaled_ref, square_ref, sum_ref, cosine_ref, sine_ref,
    kv_out, q_out, kv_all, q_all, vt_ref, qb_ref, top_ref, acc_ref, att_out, attended_ref,
    mq_ref, mk_ref, mv_ref, pre_ref, states_ref, prefix_in, prefix_out, enter_ref,
    inner_ref, inner_den, inner_top, cumulative_ref, offset_ref, memory_ref,
    part_ref, pair_in, line_out, line_in,
    load_sems, line_send, line_recv, pair_send, pair_recv,
    kv_send, fwd_send, kv_recv, q_send, q_recv, att_send, att_recv,
    st_send, st_recv, px_send, px_recv,
    sp_send, sp_recv, sl_send, sl_recv,
):
    rows, columns = shard_ref.shape
    features = x_ref.shape[1]
    width = mq_ref.shape[1]
    heads = width // HEAD
    groups = width // 128
    lines = size // CORES
    spans = depth * across
    parts = spans // heads
    span = rows // chunks
    packed = span // 2

    tp = lax.axis_index("tp")
    core = lax.rem(tp, CORES)
    line = tp // CORES
    pair = line * CORES + (1 - core)
    me = lax.axis_index("sp")
    z = me // across
    x = lax.rem(me, across)
    my_head = me // parts
    my_part = lax.rem(me, parts)

    def owner_of(place):
        place_part = lax.rem(place, parts)
        return jnp.where((place // parts) % 2 == 0, place_part, parts - 1 - place_part)

    loads = []
    for place, (source, target) in enumerate(
        ((wk, sk), (wv, sv), (wq, sq), (wmk, smk), (wmv, smv), (wmq, smq), (woa, soa), (wom, som))
    ):
        copy = pltpu.make_async_copy(source, target, load_sems.at[place])
        copy.start()
        loads.append(copy)

    barrier = pltpu.get_barrier_semaphore()
    signal(barrier, "tp", pair)
    for step in range(1, lines):
        signal(barrier, "tp", lax.rem(line + step, lines) * CORES + core)
    for step in range(1, spans):
        signal(barrier, "sp", lax.rem(me + step, spans))

    cosine_ref[...] = jnp.concatenate([cos_ref[...]] * (128 * 2 // DD), axis=0).T
    sine_ref[...] = jnp.concatenate([-sin_ref[...], sin_ref[...]] * (128 // DD), axis=0).T
    lanes = lax.broadcasted_iota(jnp.int32, (1, 128), 1)
    former = lax.rem(lanes, DD) < DD // 2
    low_lanes = lanes < HEAD

    def columns_of(owner):
        return pl.ds(pl.multiple_of(owner * columns, 128), columns)

    def rows_of(chunk):
        return pl.ds(chunk * span, span)

    def place(owner, chunk):
        return x_ref.at[rows_of(chunk), columns_of(owner)]

    pl.semaphore_wait(barrier, lines + spans - 1)

    sends = []
    pairs = {}
    for chunk in range(chunks):
        for step in range(1, lines):
            copy = remote(
                shard_ref.at[rows_of(chunk)], place(tp, chunk), line_send.at[step, chunk],
                line_recv.at[step, chunk], "tp", lax.rem(line + step, lines) * CORES + core,
            )
            copy.start()
            sends.append(copy)
    for chunk in range(chunks):
        copy = remote(
            shard_ref.at[rows_of(chunk)], place(tp, chunk), pair_send.at[0, chunk],
            pair_recv.at[0, chunk], "tp", pair,
        )
        copy.start()
        pairs[0, chunk] = copy

    def take(values, at_rows, owner):
        floats = values.astype(jnp.float32)
        scaled_ref[at_rows, columns_of(owner)] = (floats * gain_ref[:, columns_of(owner)]).astype(
            jnp.bfloat16
        )
        return jnp.sum(floats * floats, axis=1, keepdims=True)

    everywhere = pl.ds(0, rows)
    squares = take(shard_ref[...], everywhere, tp)
    for chunk in range(chunks):
        pairs[0, chunk].wait_recv()
    square_ref[...] = squares + take(x_ref[:, columns_of(pair)], everywhere, pair)

    def line_columns(owner_line):
        return pl.ds(pl.multiple_of(owner_line * CORES * columns, 128), CORES * columns)

    weights = (sk, sv, sq, smk, smv, smq)
    for index, weight in enumerate(weights):
        loads[index].wait()
        sum_ref[:, index * width : (index + 1) * width] = dot(
            scaled_ref[:, line_columns(line)], weight[line_columns(line), :]
        )

    gate_weights = jnp.concatenate([wi[...], wf[...]], axis=0)
    factor = (DD**-0.5) * LOG2E

    def rotated(wide, cosine, sine):
        partner = jnp.where(former, pltpu.roll(wide, 128 - DD // 2, 1), pltpu.roll(wide, DD // 2, 1))
        return wide * cosine + partner * sine

    def kv_sends(chunk):
        for rank in range(heads - 1, 0, -1):
            head = near_first(my_head, heads, rank)
            yield remote(
                kv_out.at[head, rows_of(chunk)], kv_all.at[me, rows_of(chunk)],
                kv_send.at[rank, chunk], kv_recv.at[me, chunk], "sp", head * parts + my_part,
            )

    def forwards(source, origin, index, chunk):
        for step in range(1, parts):
            yield remote(
                source, kv_all.at[origin, rows_of(chunk)], fwd_send.at[index, step, chunk],
                kv_recv.at[origin, chunk], "sp",
                my_head * parts + lax.rem(my_part + step, parts),
            )

    packed_of = lambda chunk: pl.ds(chunk * packed, packed)
    my_slot = me // parts
    my_owner = owner_of(me)

    def q_sends(chunk):
        for rank in range(heads - 1, 0, -1):
            head = near_first(my_head, heads, rank)
            yield remote(
                q_out.at[head, packed_of(chunk)], q_all.at[my_slot, packed_of(chunk)],
                q_send.at[rank, chunk], q_recv.at[my_slot, chunk], "sp", head * parts + my_owner,
            )

    def q_aside(chunk):
        return remote(
            q_out.at[my_head, packed_of(chunk)], q_all.at[my_slot, packed_of(chunk)],
            q_send.at[0, chunk], q_recv.at[my_slot, chunk], "sp", my_head * parts + my_owner,
        )

    for chunk in range(chunks):
        at = rows_of(chunk)
        for step in range(1, lines):
            source = lax.rem(line + lines - step, lines) * CORES + core
            remote(
                place(source, chunk), place(source, chunk), line_send.at[step, chunk],
                line_recv.at[step, chunk], "tp", pair,
            ).wait_recv()
            copy = remote(
                place(source, chunk), place(source, chunk), pair_send.at[step, chunk],
                pair_recv.at[step, chunk], "tp", pair,
            )
            copy.start()
            pairs[step, chunk] = copy
        squares = square_ref[at]
        for step in range(1, lines):
            source = lax.rem(line + lines - step, lines) * CORES + core
            squares = squares + take(x_ref[at, columns_of(source)], at, source)
        for step in range(1, lines):
            source = lax.rem(line + lines - step, lines) * CORES + 1 - core
            pairs[step, chunk].wait_recv()
            squares = squares + take(x_ref[at, columns_of(source)], at, source)
        inverse = lax.rsqrt(squares / features + EPSILON)

        def product(index):
            total = sum_ref[at, index * width : (index + 1) * width]
            for step in range(1, lines):
                other = line_columns(lax.rem(line + step, lines))
                total = total + dot(scaled_ref[at, other], weights[index][other, :])
            return (total * inverse).astype(jnp.bfloat16).astype(jnp.float32)

        cosine = cosine_ref[at]
        sine = sine_ref[at]
        keys = product(0)
        values = product(1)
        for group in range(groups):
            lane_group = slice(group * 128, group * 128 + 128)
            key = rotated(keys[:, lane_group], cosine, sine)
            value = values[:, lane_group]
            kv_out[2 * group, at] = jnp.where(low_lanes, key, pltpu.roll(value, HEAD, 1)).astype(
                jnp.bfloat16
            )
            kv_out[2 * group + 1, at] = jnp.where(
                low_lanes, pltpu.roll(key, HEAD, 1), value
            ).astype(jnp.bfloat16)
        for copy in kv_sends(chunk):
            copy.start()
        for copy in forwards(kv_out.at[my_head, at], me, my_head, chunk):
            copy.start()
        kv_all[me, at] = kv_out[my_head, at]

        queries = product(2)
        for group in range(groups):
            query = rotated(queries[:, group * 128 : group * 128 + 128], cosine, sine) * factor
            top, bottom = query[:packed], query[packed:]
            q_out[2 * group, packed_of(chunk)] = jnp.where(
                low_lanes, top, pltpu.roll(bottom, HEAD, 1)
            ).astype(jnp.bfloat16)
            q_out[2 * group + 1, packed_of(chunk)] = jnp.where(
                low_lanes, pltpu.roll(top, HEAD, 1), bottom
            ).astype(jnp.bfloat16)
        for copy in q_sends(chunk):
            copy.start()

        @pl.when(my_owner == my_part)
        def _():
            q_all[my_slot, packed_of(chunk)] = q_out[my_head, packed_of(chunk)]

        @pl.when(my_owner != my_part)
        def _():
            q_aside(chunk).start()

        mk_ref[at] = product(3).astype(jnp.bfloat16)
        mv_ref[at] = product(4).astype(jnp.bfloat16)
        mq_ref[at] = product(5).astype(jnp.bfloat16)
        pre_ref[at, : 2 * heads] = dot(scaled_ref[at, :], gate_weights, ((1,), (1,))) * inverse

    gate = pre_ref[:, :heads]
    pre = pre_ref[:, heads : 2 * heads] + bias_ref[...]
    shift = shift_ref[...]
    shift = jnp.concatenate(
        [shift, jnp.zeros((128 - shift.shape[0], rows), jnp.float32)], axis=0
    ).T[:, : shift.shape[0]]
    forget = jnp.minimum(pre, 0.0) - jnp.log1p(jnp.exp(-jnp.abs(pre))) + shift
    row_index = lax.broadcasted_iota(jnp.int32, (rows, rows), 0)
    column_index = lax.broadcasted_iota(jnp.int32, (rows, rows), 1)
    lower = column_index <= row_index
    lower_ones = lower.astype(jnp.bfloat16)
    first, rest = two_parts(forget)
    second = (forget - first.astype(jnp.float32) - rest.astype(jnp.float32)).astype(jnp.bfloat16)
    cumulative = dot(lower_ones, first) + (dot(lower_ones, rest) + dot(lower_ones, second))
    cumulative_ref[:, :heads] = cumulative
    offsets = jnp.concatenate(
        [gate - cumulative, jnp.zeros((rows, 128 - heads), jnp.float32)], axis=1
    )
    offset_ref[...] = offsets.T[:8, :]
    end = cumulative[rows - 1 : rows, :]
    toward = end - cumulative + gate
    top = jnp.max(toward, axis=0, keepdims=True)
    end_weights = spread(jnp.exp(toward - top), width)
    keyed = mk_ref[...].astype(jnp.float32) * (HEAD**-0.5) * end_weights
    high, low = two_parts(keyed)
    whole = dot(high, mv_ref[...], ((0,), (0,))) + dot(low, mv_ref[...], ((0,), (0,)))
    memory = jnp.zeros((HEAD, width), jnp.float32)
    for head in range(heads):
        memory = jnp.where(
            head_mask(width, head), whole[head * HEAD : (head + 1) * HEAD, :], memory
        )
    states_ref[x, :HEAD, :] = memory
    states_ref[x, HEAD : HEAD + 1, :] = jnp.sum(keyed, axis=0, keepdims=True)
    states_ref[x, HEAD + 1 : HEAD + 2, :] = spread(top, width)
    states_ref[x, HEAD + 2 : HEAD + 3, :] = spread(end, width)
    states_ref[x, HEAD + 3 :, :] = jnp.zeros((STATE_ROWS - HEAD - 3, width), jnp.float32)

    def state_sends():
        for step in range(1, across):
            yield remote(
                states_ref.at[x], states_ref.at[x], st_send.at[step], st_recv.at[x], "sp",
                z * across + lax.rem(x + step, across),
            )

    for copy in state_sends():
        copy.start()

    for group in range(groups):
        lane_group = slice(group * 128, (group + 1) * 128)
        keys = mk_ref[:, lane_group]
        values = mv_ref[:, lane_group]
        group_queries = mq_ref[:, lane_group]
        result = None
        for side in range(2):
            head = group * 2 + side
            chosen = (lanes // HEAD) == side
            column = cumulative[:, head : head + 1]
            gaps = jnp.where(lower, column + offset_ref[head : head + 1, :], NEGATIVE)
            row_top = jnp.max(gaps, axis=1, keepdims=True)
            within = jnp.exp(gaps - row_top)
            scores = dot(jnp.where(chosen, group_queries, 0), keys, ((1,), (1,)))
            scores = jnp.where(lower, within * (scores * (HEAD**-0.5)), 0.0)
            inner_den[:, head : head + 1] = jnp.sum(scores, axis=1, keepdims=True)
            inner_top[:, head : head + 1] = row_top
            score_high, score_low = two_parts(scores)
            numerator = dot(score_high, values) + dot(score_low, values)
            result = numerator if result is None else jnp.where(chosen, numerator, result)
        inner_ref[:, lane_group] = result

    def advance(body, stable, later):
        later_top = later[HEAD + 1 : HEAD + 2, :]
        decay = later[HEAD + 2 : HEAD + 3, :]
        new = jnp.maximum(decay + stable, later_top)
        return jnp.exp(decay + stable - new) * body + jnp.exp(later_top - new) * later, new

    def prefix_send():
        return remote(
            prefix_out, prefix_in, px_send, px_recv, "sp", jnp.minimum(me + across, spans - 1)
        )

    def level(body, stable):
        for other in range(across):

            @pl.when(x == other)
            def _():
                enter_ref[...] = body
                enter_ref[HEAD + 1 : HEAD + 2, :] = stable

            if other < across - 1:
                body, stable = advance(body, stable, states_ref[other])
        body, stable = advance(body, stable, states_ref[across - 1])

        @pl.when(z < depth - 1)
        def _():
            prefix_out[...] = body
            prefix_out[HEAD + 1 : HEAD + 2, :] = stable
            prefix_send().start()

    for step in range(1, across):
        other = lax.rem(x + step, across)
        remote(
            states_ref.at[other], states_ref.at[other], st_send.at[step], st_recv.at[other], "sp", me
        ).wait_recv()

    @pl.when(z == 0)
    def _():
        level(jnp.zeros((STATE_ROWS, width), jnp.float32), jnp.zeros((1, width), jnp.float32))

    def chain():
        prefix_send().wait_recv()
        body = prefix_in[...]
        level(body, body[HEAD + 1 : HEAD + 2, :])

    top_ref[...] = jnp.full(top_ref.shape, NEGATIVE, jnp.float32)
    acc_ref[...] = jnp.zeros(acc_ref.shape, jnp.float32)
    query_width = 2 * rows
    tiles = [slice(start, min(start + TILE, query_width)) for start in range(0, query_width, TILE)]

    def block(slot, place, diagonal):
        def score(tile):
            scores = dot(kv_all[place], qb_ref[slot, tile], ((1,), (1,)))
            if diagonal:
                shape = scores.shape
                key_index = lax.broadcasted_iota(jnp.int32, shape, 0)
                query_index = lax.broadcasted_iota(jnp.int32, shape, 1) + tile.start
                query_index = jnp.where(query_index >= rows, query_index - rows, query_index)
                scores = jnp.where(key_index <= query_index, scores, NEGATIVE)
            return scores

        def soften(tile, scores):
            old_top = top_ref[slot, :, tile]
            top = jnp.maximum(jnp.max(scores, axis=0, keepdims=True), old_top)
            return top, jnp.exp2(old_top - top), jnp.exp2(scores - top).astype(jnp.bfloat16)

        def gather_up(tile, top, shrink, weights):
            sums = dot(vt_ref[place], weights)
            acc_ref[slot, :, tile] = acc_ref[slot, :, tile] * shrink + sums
            top_ref[slot, :, tile] = top

        scores = score(tiles[0])
        held = None
        for index, tile in enumerate(tiles):
            following = score(tiles[index + 1]) if index + 1 < len(tiles) else None
            if held is not None:
                gather_up(tiles[index - 1], *held)
            held = soften(tile, scores)
            scores = following
        gather_up(tiles[-1], *held)

    def visit_place(rank):
        level_rank = rank // across
        return near_first(z, depth, level_rank) * across + lax.rem(
            x + lax.rem(rank, across), across
        )

    def arrive(origin):
        for chunk in range(chunks):
            remote(
                kv_all.at[origin, rows_of(chunk)], kv_all.at[origin, rows_of(chunk)],
                kv_send.at[0, chunk], kv_recv.at[origin, chunk], "sp", me,
            ).wait_recv()

            @pl.when(lax.rem(origin, parts) == my_part)
            def _():
                for copy in forwards(
                    kv_all.at[origin, rows_of(chunk)], origin, origin // parts, chunk
                ):
                    copy.start()

    def visit(rank, unused):
        origin = visit_place(rank)
        slot = origin // parts
        owned = owner_of(origin) == my_part
        pl.when(origin != me)(lambda: arrive(origin))
        turned = kv_all[origin].T
        vt_ref[origin, :HEAD, :] = turned[HEAD:, :]
        vt_ref[origin, HEAD:, :] = jnp.ones((VALUE_ROWS - HEAD, rows), jnp.bfloat16)

        @pl.when(owned)
        def _():
            @pl.when(origin != me)
            def _():
                for chunk in range(chunks):
                    at = q_all.at[slot, packed_of(chunk)]
                    remote(
                        at, at, q_send.at[0, chunk], q_recv.at[slot, chunk], "sp", me
                    ).wait_recv()

            for chunk in range(chunks):
                low_rows = q_all[slot, packed_of(chunk)].astype(jnp.float32)
                high_rows = pltpu.roll(low_rows, HEAD, 1)
                for half in range(2):
                    chosen = (lanes // DD) == half
                    for side, values in enumerate((low_rows, high_rows)):
                        qb_ref[
                            slot, pl.ds(half * rows + chunk * span + side * packed, packed)
                        ] = jnp.where(chosen, values, 0.0).astype(jnp.bfloat16)

            block(slot, origin, True)

        def earlier(other_rank, unused):
            other = visit_place(other_rank)
            query = jnp.maximum(origin, other)
            key = jnp.minimum(origin, other)

            @pl.when(owner_of(query) == my_part)
            def _():
                block(query // parts, key, False)

            return unused

        lax.fori_loop(0, rank, earlier, 0)
        pl.when((z > 0) & (rank == 2 * z - 1))(chain)
        return unused

    lax.fori_loop(0, spans, visit, 0)

    eye = lax.broadcasted_iota(jnp.int32, (HEAD, HEAD), 0) == lax.broadcasted_iota(
        jnp.int32, (HEAD, HEAD), 1
    )
    head_gain = jnp.sum(jnp.where(eye, head_gain_ref[...], 0.0), axis=1, keepdims=True)
    head_lanes = lax.broadcasted_iota(jnp.int32, lambda_ref.shape, 1)
    factor_second = jnp.sum(
        jnp.where(head_lanes == my_head, lambda_ref[...], 0.0), axis=1, keepdims=True
    )

    def span_of(slot):
        return slot * parts + (my_part if slot % 2 == 0 else parts - 1 - my_part)

    def att_copy(slot):
        return remote(
            att_out.at[slot], attended_ref.at[pl.ds(pl.multiple_of(my_head * HEAD, HEAD), HEAD)],
            att_send.at[slot], att_recv.at[my_head], "sp", span_of(slot),
        )

    for slot in range(heads):
        first, second = (
            acc_ref[slot, :HEAD, half * rows : (half + 1) * rows]
            / acc_ref[slot, HEAD : HEAD + 1, half * rows : (half + 1) * rows]
            for half in range(2)
        )
        difference = first - factor_second * second
        mean = jnp.mean(difference * difference, axis=0, keepdims=True)
        att_out[slot] = (difference * lax.rsqrt(mean + EPSILON) * head_gain).astype(jnp.bfloat16)

        @pl.when(span_of(slot) == me)
        def _():
            attended_ref[pl.ds(pl.multiple_of(my_head * HEAD, HEAD), HEAD), :] = att_out[slot]

        @pl.when(span_of(slot) != me)
        def _():
            att_copy(slot).start()

    stable = enter_ref[HEAD + 1 : HEAD + 2, :]
    memory_in = enter_ref[:HEAD, :]
    normal_in = enter_ref[HEAD : HEAD + 1, :]
    blocks = jnp.concatenate(
        [jnp.where(head_mask(width, head), memory_in, 0.0) for head in range(heads)], axis=0
    )
    high, low = two_parts(blocks)
    memory_queries = mq_ref[...]
    carried_part = dot(memory_queries, high) + dot(memory_queries, low)
    weighted = memory_queries.astype(jnp.float32) * normal_in
    for group in range(groups):
        lane_group = slice(group * 128, (group + 1) * 128)
        result = None
        for side in range(2):
            head = group * 2 + side
            chosen = (lanes // HEAD) == side
            column = slice(head, head + 1)
            carried_log = cumulative_ref[:, column] + stable[:, head * HEAD : head * HEAD + 1]
            own_top = inner_top[:, column]
            row_top = jnp.maximum(carried_log, own_top)
            inside = jnp.exp(own_top - row_top)
            outside = jnp.exp(carried_log - row_top)
            denominator = inside * inner_den[:, column] + outside * jnp.sum(
                jnp.where(chosen, weighted[:, lane_group], 0.0), axis=1, keepdims=True
            )
            numerator = inside * inner_ref[:, lane_group] + outside * carried_part[:, lane_group]
            quotient = numerator / jnp.maximum(jnp.abs(denominator), 1.0)
            result = quotient if result is None else jnp.where(chosen, quotient, result)
        memory_ref[:, lane_group] = result.astype(jnp.bfloat16)

    loads[6].wait()
    loads[7].wait()
    for step in range(heads):
        here = (my_owner != my_part) | (my_head != step)

        @pl.when(here)
        def _():
            at = attended_ref.at[pl.ds(step * HEAD, HEAD)]
            remote(at, at, att_send.at[0], att_recv.at[step], "sp", me).wait_recv()

    out_span = rows // out_chunks

    def out_rows(chunk):
        return pl.ds(chunk * out_span, out_span)

    order = list(range(1, lines)) + [0]
    swaps = {}
    lined = {}

    def pair_sum(step, chunk):
        swaps[step, chunk].wait_recv()
        mine = part_ref[
            out_rows(chunk), columns_of(lax.rem(line + step, lines) * CORES + core)
        ]
        return mine.astype(jnp.float32) + pair_in[step, out_rows(chunk), :].astype(jnp.float32)

    def pass_on(chunk):
        for step in range(1, lines):
            line_out[step, out_rows(chunk), :] = pair_sum(step, chunk).astype(jnp.bfloat16)
            copy = remote(
                line_out.at[step, out_rows(chunk)], line_in.at[step, out_rows(chunk)],
                sl_send.at[step, chunk], sl_recv.at[step, chunk], "tp",
                lax.rem(line + step, lines) * CORES + core,
            )
            copy.start()
            lined[step, chunk] = copy

    for chunk in range(out_chunks):
        at = slice(chunk * out_span, (chunk + 1) * out_span)
        part_ref[at, :] = (
            dot(attended_ref[:, at], soa[...], ((0,), (0,))) + dot(memory_ref[at, :], som[...])
        ).astype(jnp.bfloat16)
        for step in order:
            target = lax.rem(line + step, lines) * CORES + (1 - core)
            copy = remote(
                part_ref.at[out_rows(chunk), columns_of(target)],
                pair_in.at[step, out_rows(chunk)], sp_send.at[step, chunk],
                sp_recv.at[step, chunk], "tp", pair,
            )
            copy.start()
            swaps[step, chunk] = copy
        if chunk > 0:
            pass_on(chunk - 1)
    pass_on(out_chunks - 1)

    for copy in sends:
        copy.wait_send()
    for copy in pairs.values():
        copy.wait_send()
    for chunk in range(chunks):
        for copy in kv_sends(chunk):
            copy.wait_send()
        for copy in q_sends(chunk):
            copy.wait_send()
        for index in range(heads):
            for copy in forwards(kv_all.at[0, rows_of(chunk)], 0, index, chunk):
                copy.wait_send()

        @pl.when(my_owner != my_part)
        def _():
            q_aside(chunk).wait_send()

    for copy in state_sends():
        copy.wait_send()
    pl.when(z < depth - 1)(lambda: prefix_send().wait_send())
    for slot in range(heads):

        @pl.when(span_of(slot) != me)
        def _():
            att_copy(slot).wait_send()

    for chunk in range(out_chunks):
        total = pair_sum(0, chunk)
        for step in range(1, lines):
            lined[step, chunk].wait_recv()
            total = total + line_in[step, out_rows(chunk), :].astype(jnp.float32)
        out_ref[out_rows(chunk), :] = total.astype(jnp.bfloat16)
    for copy in swaps.values():
        copy.wait_send()
    for copy in lined.values():
        copy.wait_send()


def per_device(tp_size, depth, across, inputs, norm_gain, query_weight, key_weight, value_weight,
               memory_query_weight, memory_key_weight, memory_value_weight, input_gate_weight,
               forget_gate_weight, forget_bias, decay_shift, lambdas, head_gain,
               out_weight_attention, out_weight_memory):
    rows, columns = inputs.shape
    features = norm_gain.shape[0]
    width = query_weight.shape[1]
    heads = width // HEAD
    lines = tp_size // CORES
    spans = depth * across
    parts = spans // heads
    chunks = 4
    out_chunks = 3
    dma = pltpu.SemaphoreType.DMA

    middle = DD // 2
    inverse = 1.0 / ROTARY_BASE ** (jnp.arange(middle, dtype=jnp.float32) / middle)
    positions = lax.axis_index("sp") * rows + jnp.arange(rows, dtype=jnp.int32)
    angles = inverse[:, None] * positions.astype(jnp.float32)[None, :]
    cosine = jnp.cos(angles)
    sine = jnp.sin(angles)

    hbm = pl.BlockSpec(memory_space=pl.ANY)
    bf16 = lambda *shape: pltpu.VMEM(shape, jnp.bfloat16)
    f32 = lambda *shape: pltpu.VMEM(shape, jnp.float32)
    return pl.pallas_call(
        functools.partial(layer_kernel, tp_size, depth, across, chunks, out_chunks),
        out_shape=jax.ShapeDtypeStruct((rows, columns), jnp.bfloat16),
        in_specs=[VMEM] * 4 + [hbm] * 6 + [VMEM] * 6 + [hbm] * 2,
        out_specs=VMEM,
        scratch_shapes=[bf16(features, width)] * 6
        + [bf16(width, features)] * 2
        + [
            bf16(rows, features), bf16(rows, features), f32(rows, 1), f32(rows, 6 * width),
            f32(rows, 128), f32(rows, 128),
            bf16(heads, rows, 128), bf16(heads, rows // 2, 128), bf16(spans, rows, 128),
            bf16(heads, rows // 2, 128), bf16(spans, VALUE_ROWS, rows),
            bf16(heads, 2 * rows, 128), f32(heads, 1, 2 * rows), f32(heads, VALUE_ROWS, 2 * rows),
            bf16(heads, HEAD, rows), bf16(width, rows),
            bf16(rows, width), bf16(rows, width), bf16(rows, width), f32(rows, 128),
            f32(across, STATE_ROWS, width), f32(STATE_ROWS, width), f32(STATE_ROWS, width),
            f32(STATE_ROWS, width),
            f32(rows, width), f32(rows, 128), f32(rows, 128), f32(rows, 128), f32(8, rows),
            bf16(rows, width),
            bf16(rows, features), bf16(lines, rows, columns), bf16(lines, rows, columns),
            bf16(lines, rows, columns),
            dma((8,)), dma((lines, chunks)), dma((lines, chunks)), dma((lines, chunks)),
            dma((lines, chunks)),
            dma((heads, chunks)), dma((heads, parts, chunks)), dma((spans, chunks)),
            dma((heads, chunks)), dma((heads, chunks)), dma((heads,)), dma((heads,)),
            dma((across,)), dma((across,)), dma(()), dma(()),
            dma((lines, out_chunks)), dma((lines, out_chunks)), dma((lines, out_chunks)),
            dma((lines, out_chunks)),
        ],
        compiler_params=pltpu.CompilerParams(
            vmem_limit_bytes=VMEM_LIMIT, collective_id=0, has_side_effects=True
        ),
        name="layer",
    )(
        inputs, norm_gain[None, :], cosine, sine, query_weight, key_weight, value_weight,
        memory_query_weight, memory_key_weight, memory_value_weight, input_gate_weight.T,
        forget_gate_weight.T, forget_bias[None, :], decay_shift.T, lambdas[None, :],
        head_gain[None, :], out_weight_attention, out_weight_memory,
    )


def columns_across(mesh):
    spans = mesh.shape["sp"]
    try:
        places = {device.coords[0] for device in mesh.devices.flat}
        across = len(places)
    except AttributeError:
        across = 2
    return across if spans % across == 0 else 1


def solution(mesh):
    across = columns_across(mesh)
    in_specs = (
        P("sp", "tp"),
        P(),
        P(None, "tp"),
        P(None, "tp"),
        P(None, "tp"),
        P(None, "tp"),
        P(None, "tp"),
        P(None, "tp"),
        P(None, "tp"),
        P(None, "tp"),
        P("tp"),
        P("sp", "tp"),
        P("tp"),
        P(),
        P("tp", None),
        P("tp", None),
    )
    return jax.shard_map(
        functools.partial(
            per_device, mesh.shape["tp"], mesh.shape["sp"] // across, across
        ),
        mesh=mesh,
        in_specs=in_specs,
        out_specs=P("sp", "tp"),
        check_vma=False,
    )
```

time: 94.6 us -> 69.8 us (0.74)
  the two profiles are of different devices: /device:TPU:25 before, /device:TPU:0 now
where the time goes in v1:
time: 69.8 us; the launch traced here: 69.6 us
  Pallas kernels  67 us (96%)
  local copies, waits for them, and re-layouts  1.77 us (3%)
  other arithmetic  0.82 us (1%)
    pallas_call x1, Pallas kernels, per_device(): pl.pallas_call(functools.partial(layer_kernel, tp_size, depth, across, ch...  67 us
    unnamed x1, local copies, waits for them, and re-layouts  1.77 us

profile of v1, /device:TPU:0, one launch (start us, length us, event | category | flops | bytes accessed | tf_op | source)
XLA Modules:
  0.0 69.6 jit_solution(14489064303788119762)
XLA Ops:
  0.0 0.8 %multiply_sine_fusion = (f32[16,384]{1,0:T(8,128)}, f32[16,384]{1,0:T(8,128)}) fusion(f32[384]{0:T(512)S(1)} %add_convert_fusion, f32[16]{0:T(128)S(1)} %negate_power_fusion), kind=kLoop, calls=%fused_computation | loop fusion | flops 6144 | bytes 50752 | tf_op jit(solution)/shard_map/sin | solution.py:697
  0.8 67.0 %layer.1 = bf16[384,512]{1,0:T(8,128)(2,1)} custom-call(bf16[384,512]{1,0:T(8,128)(2,1)} %shard_ref.1, f32[1,2048]{1,0:T(1,128)} %bitcast.9, f32[16,384]{1,0:T(8,128)} %get-tuple-element.6.cos_ref, f32[16,384]{1,0:T(8,128)} %get-tuple-element.5.sin_ref, bf16[2048,256]{1,0:T(8,128)(2,1)} %wq.1, bf16[2048,256]{1,0:T(8,128)(2,1)} %wk.1, bf16[2048,256]{1,0:T(8,128)(2,1)} %wv.1, ...), custom_call_target="tpu_custom_call" | custom-call | tf_op jit(solution)/shard_map/layer/pallas_call | solution.py:702
  67.8 1.8 %copy.18 = bf16[384,512]{1,0:T(8,128)(2,1)} copy(bf16[384,512]{1,0:T(8,128)(2,1)} %layer.1) | data formatting | bytes 786432
  (2 shorter events, 0.0 us)

commit v2 on v1

--- a/solution.py
+++ b/solution.py
@@ -19,7 +19,6 @@
 VMEM = pl.BlockSpec(memory_space=pltpu.VMEM)
 MESH = pl.DeviceIdType.MESH
 VMEM_LIMIT = 60 * 1024 * 1024
-TILE = 256
 
 
 def signal(semaphore, axis, place):
@@ -72,11 +71,11 @@
     shard_ref, gain_ref, cos_ref, sin_ref, wq, wk, wv, wmq, wmk, wmv, wi, wf, bias_ref, shift_ref,
     lambda_ref, head_gain_ref, woa, wom,
     out_ref,
-    sq, sk, sv, smq, smk, smv, soa, som, x_ref, scaled_ref, square_ref, sum_ref, cosine_ref, sine_ref,
-    kv_out, q_out, kv_all, q_all, vt_ref, qb_ref, top_ref, acc_ref, att_out, attended_ref,
+    weight_ref, soa, som, x_ref, scaled_ref, square_ref, sum_ref, cosine_ref, sine_ref,
+    kv_out, q_out, kv_all, q_all, vt_ref, qn_ref, qt_ref, top_ref, acc_ref, att_out, attended_ref,
     mq_ref, mk_ref, mv_ref, pre_ref, states_ref, prefix_in, prefix_out, enter_ref,
     inner_ref, inner_den, inner_top, cumulative_ref, offset_ref, memory_ref,
-    part_ref, pair_in, line_out, line_in,
+    partial_ref, part_ref, pair_in, line_out, line_in,
     load_sems, line_send, line_recv, pair_send, pair_recv,
     kv_send, fwd_send, kv_recv, q_send, q_recv, att_send, att_recv,
     st_send, st_recv, px_send, px_recv,
@@ -108,12 +107,16 @@
         return jnp.where((place // parts) % 2 == 0, place_part, parts - 1 - place_part)
 
     loads = []
-    for place, (source, target) in enumerate(
-        ((wk, sk), (wv, sv), (wq, sq), (wmk, smk), (wmv, smv), (wmq, smq), (woa, soa), (wom, som))
-    ):
-        copy = pltpu.make_async_copy(source, target, load_sems.at[place])
+    for index, source in enumerate((wk, wv, wq, wmk, wmv, wmq)):
+        loads.append(
+            pltpu.make_async_copy(
+                source, weight_ref.at[:, pl.ds(index * width, width)], load_sems.at[index]
+            )
+        )
+    loads.append(pltpu.make_async_copy(woa, soa, load_sems.at[6]))
+    loads.append(pltpu.make_async_copy(wom, som, load_sems.at[7]))
+    for copy in loads:
         copy.start()
-        loads.append(copy)
 
     barrier = pltpu.get_barrier_semaphore()
     signal(barrier, "tp", pair)
@@ -173,11 +176,12 @@
     def line_columns(owner_line):
         return pl.ds(pl.multiple_of(owner_line * CORES * columns, 128), CORES * columns)
 
-    weights = (sk, sv, sq, smk, smv, smq)
-    for index, weight in enumerate(weights):
-        loads[index].wait()
-        sum_ref[:, index * width : (index + 1) * width] = dot(
-            scaled_ref[:, line_columns(line)], weight[line_columns(line), :]
+    couples = [slice(index * width, (index + 2) * width) for index in (0, 2, 4)]
+    for index, couple in enumerate(couples):
+        loads[2 * index].wait()
+        loads[2 * index + 1].wait()
+        sum_ref[:, couple] = dot(
+            scaled_ref[:, line_columns(line)], weight_ref[line_columns(line), couple]
         )
 
     gate_weights = jnp.concatenate([wi[...], wf[...]], axis=0)
@@ -202,6 +206,27 @@
                 kv_recv.at[origin, chunk], "sp",
                 my_head * parts + lax.rem(my_part + step, parts),
             )
+
+    points = {
+        (1, 0): "chunk2", (2, 0): "projected", (3, 0): "projected", (1, 1): "projected",
+        (2, 1): "state", (1, 2): "state", (3, 1): "inner", (2, 2): "inner", (1, 3): "inner",
+        (3, 2): "first", (2, 3): "second", (3, 3): "seconded",
+    }
+
+    def landed(rank):
+        return near_first(my_head, heads, rank) * parts + my_part
+
+    def forward(point, index=""):
+        for chunk in range(chunks):
+            for rank in range(1, heads):
+                if points.get((rank, chunk), "inner") == f"{point}{index}":
+                    origin = landed(rank)
+                    at = kv_all.at[origin, rows_of(chunk)]
+                    remote(
+                        at, at, kv_send.at[0, chunk], kv_recv.at[origin, chunk], "sp", me
+                    ).wait_recv()
+                    for copy in forwards(at, origin, origin // parts, chunk):
+                        copy.start()
 
     packed_of = lambda chunk: pl.ds(chunk * packed, packed)
     my_slot = me // parts
@@ -245,17 +270,17 @@
             squares = squares + take(x_ref[at, columns_of(source)], at, source)
         inverse = lax.rsqrt(squares / features + EPSILON)
 
-        def product(index):
-            total = sum_ref[at, index * width : (index + 1) * width]
+        def products(index):
+            total = sum_ref[at, couples[index]]
             for step in range(1, lines):
                 other = line_columns(lax.rem(line + step, lines))
-                total = total + dot(scaled_ref[at, other], weights[index][other, :])
-            return (total * inverse).astype(jnp.bfloat16).astype(jnp.float32)
+                total = total + dot(scaled_ref[at, other], weight_ref[other, couples[index]])
+            total = (total * inverse).astype(jnp.bfloat16).astype(jnp.float32)
+            return total[:, :width], total[:, width:]
 
         cosine = cosine_ref[at]
         sine = sine_ref[at]
-        keys = product(0)
-        values = product(1)
+        keys, values = products(0)
         for group in range(groups):
             lane_group = slice(group * 128, group * 128 + 128)
             key = rotated(keys[:, lane_group], cosine, sine)
@@ -272,7 +297,7 @@
             copy.start()
         kv_all[me, at] = kv_out[my_head, at]
 
-        queries = product(2)
+        queries, memory_keys = products(1)
         for group in range(groups):
             query = rotated(queries[:, group * 128 : group * 128 + 128], cosine, sine) * factor
             top, bottom = query[:packed], query[packed:]
@@ -293,10 +318,15 @@
         def _():
             q_aside(chunk).start()
 
-        mk_ref[at] = product(3).astype(jnp.bfloat16)
-        mv_ref[at] = product(4).astype(jnp.bfloat16)
-        mq_ref[at] = product(5).astype(jnp.bfloat16)
+        mk_ref[at] = memory_keys.astype(jnp.bfloat16)
+        memory_values, memory_queries = products(2)
+        mv_ref[at] = memory_values.astype(jnp.bfloat16)
+        mq_ref[at] = memory_queries.astype(jnp.bfloat16)
         pre_ref[at, : 2 * heads] = dot(scaled_ref[at, :], gate_weights, ((1,), (1,))) * inverse
+        if chunk < chunks - 1:
+            forward("chunk", chunk)
+
+    forward("projected")
 
     gate = pre_ref[:, :heads]
     pre = pre_ref[:, heads : 2 * heads] + bias_ref[...]
@@ -345,6 +375,7 @@
     for copy in state_sends():
         copy.start()
 
+    forward("state")
     for group in range(groups):
         lane_group = slice(group * 128, (group + 1) * 128)
         keys = mk_ref[:, lane_group]
@@ -367,6 +398,7 @@
             result = numerator if result is None else jnp.where(chosen, numerator, result)
         inner_ref[:, lane_group] = result
 
+    forward("inner")
     def advance(body, stable, later):
         later_top = later[HEAD + 1 : HEAD + 2, :]
         decay = later[HEAD + 2 : HEAD + 3, :]
@@ -396,88 +428,78 @@
             prefix_out[HEAD + 1 : HEAD + 2, :] = stable
             prefix_send().start()
 
-    for step in range(1, across):
-        other = lax.rem(x + step, across)
-        remote(
-            states_ref.at[other], states_ref.at[other], st_send.at[step], st_recv.at[other], "sp", me
-        ).wait_recv()
-
-    @pl.when(z == 0)
-    def _():
-        level(jnp.zeros((STATE_ROWS, width), jnp.float32), jnp.zeros((1, width), jnp.float32))
-
     def chain():
-        prefix_send().wait_recv()
+        for step in range(1, across):
+            other = lax.rem(x + step, across)
+            at = states_ref.at[other]
+            remote(at, at, st_send.at[step], st_recv.at[other], "sp", me).wait_recv()
+
+        @pl.when(z == 0)
+        def _():
+            prefix_in[...] = jnp.zeros((STATE_ROWS, width), jnp.float32)
+
+        pl.when(z > 0)(lambda: prefix_send().wait_recv())
         body = prefix_in[...]
         level(body, body[HEAD + 1 : HEAD + 2, :])
 
     top_ref[...] = jnp.full(top_ref.shape, NEGATIVE, jnp.float32)
     acc_ref[...] = jnp.zeros(acc_ref.shape, jnp.float32)
-    query_width = 2 * rows
-    tiles = [slice(start, min(start + TILE, query_width)) for start in range(0, query_width, TILE)]
-
-    def block(slot, place, diagonal):
-        def score(tile):
-            scores = dot(kv_all[place], qb_ref[slot, tile], ((1,), (1,)))
-            if diagonal:
-                shape = scores.shape
-                key_index = lax.broadcasted_iota(jnp.int32, shape, 0)
-                query_index = lax.broadcasted_iota(jnp.int32, shape, 1) + tile.start
-                query_index = jnp.where(query_index >= rows, query_index - rows, query_index)
-                scores = jnp.where(key_index <= query_index, scores, NEGATIVE)
-            return scores
-
-        def soften(tile, scores):
-            old_top = top_ref[slot, :, tile]
+    units = spans // 2
+    half_rows = rows // 2
+
+    def run(steps):
+        def score(step):
+            slot, wave, place, diagonal = step
+            if not diagonal:
+                return dot(kv_all[place], qt_ref[slot, wave])
+            visible = (wave + 1) * half_rows
+            scores = dot(kv_all[place, :visible], qt_ref[slot, wave])
+            key_index = lax.broadcasted_iota(jnp.int32, scores.shape, 0)
+            query_index = lax.broadcasted_iota(jnp.int32, scores.shape, 1)
+            query_index = jnp.where(query_index >= half_rows, query_index - half_rows, query_index)
+            return jnp.where(key_index <= query_index + wave * half_rows, scores, NEGATIVE)
+
+        def soften(step, scores):
+            slot, wave, place, diagonal = step
+            old_top = top_ref[slot, wave]
             top = jnp.maximum(jnp.max(scores, axis=0, keepdims=True), old_top)
-            return top, jnp.exp2(old_top - top), jnp.exp2(scores - top).astype(jnp.bfloat16)
-
-        def gather_up(tile, top, shrink, weights):
-            sums = dot(vt_ref[place], weights)
-            acc_ref[slot, :, tile] = acc_ref[slot, :, tile] * shrink + sums
-            top_ref[slot, :, tile] = top
-
-        scores = score(tiles[0])
+            top_ref[slot, wave] = top
+            return jnp.exp2(old_top - top), jnp.exp2(scores - top).astype(jnp.bfloat16)
+
+        def gather_up(step, shrink, weights):
+            slot, wave, place, diagonal = step
+            sums = dot(vt_ref[place, :, : weights.shape[0]], weights)
+            acc_ref[slot, wave] = acc_ref[slot, wave] * shrink + sums
+
+        count = len(steps)
+        scores = [score(step) for step in steps[:2]]
         held = None
-        for index, tile in enumerate(tiles):
-            following = score(tiles[index + 1]) if index + 1 < len(tiles) else None
+        for index, step in enumerate(steps):
+            if index + 2 < count:
+                scores.append(score(steps[index + 2]))
             if held is not None:
-                gather_up(tiles[index - 1], *held)
-            held = soften(tile, scores)
-            scores = following
-        gather_up(tiles[-1], *held)
-
-    def visit_place(rank):
-        level_rank = rank // across
-        return near_first(z, depth, level_rank) * across + lax.rem(
-            x + lax.rem(rank, across), across
-        )
+                gather_up(steps[index - 1], *held)
+            held = soften(step, scores[index])
+        gather_up(steps[-1], *held)
+
+    def visit_unit(rank):
+        return near_first(me // 2, units, rank)
 
     def arrive(origin):
-        for chunk in range(chunks):
-            remote(
-                kv_all.at[origin, rows_of(chunk)], kv_all.at[origin, rows_of(chunk)],
-                kv_send.at[0, chunk], kv_recv.at[origin, chunk], "sp", me,
-            ).wait_recv()
-
-            @pl.when(lax.rem(origin, parts) == my_part)
-            def _():
-                for copy in forwards(
-                    kv_all.at[origin, rows_of(chunk)], origin, origin // parts, chunk
-                ):
-                    copy.start()
-
-    def visit(rank, unused):
-        origin = visit_place(rank)
-        slot = origin // parts
-        owned = owner_of(origin) == my_part
-        pl.when(origin != me)(lambda: arrive(origin))
+        @pl.when((origin != me) & (lax.rem(origin, parts) != my_part))
+        def _():
+            for chunk in range(chunks):
+                at = kv_all.at[origin, rows_of(chunk)]
+                remote(at, at, kv_send.at[0, chunk], kv_recv.at[origin, chunk], "sp", me).wait_recv()
+
         turned = kv_all[origin].T
         vt_ref[origin, :HEAD, :] = turned[HEAD:, :]
         vt_ref[origin, HEAD:, :] = jnp.ones((VALUE_ROWS - HEAD, rows), jnp.bfloat16)
 
-        @pl.when(owned)
-        def _():
+        @pl.when(owner_of(origin) == my_part)
+        def _():
+            slot = origin // parts
+
             @pl.when(origin != me)
             def _():
                 for chunk in range(chunks):
@@ -487,33 +509,71 @@
                     ).wait_recv()
 
             for chunk in range(chunks):
+                wave = chunk * span // half_rows
+                start = chunk * span - wave * half_rows
                 low_rows = q_all[slot, packed_of(chunk)].astype(jnp.float32)
                 high_rows = pltpu.roll(low_rows, HEAD, 1)
                 for half in range(2):
                     chosen = (lanes // DD) == half
                     for side, values in enumerate((low_rows, high_rows)):
-                        qb_ref[
-                            slot, pl.ds(half * rows + chunk * span + side * packed, packed)
+                        qn_ref[
+                            wave, pl.ds(half * half_rows + start + side * packed, packed)
                         ] = jnp.where(chosen, values, 0.0).astype(jnp.bfloat16)
-
-            block(slot, origin, True)
+            for wave in range(2):
+                qt_ref[slot, wave] = qn_ref[wave].T
+
+    def mine(unit):
+        return [owner_of(2 * unit + side) == my_part for side in range(2)]
+
+    def within(unit, waves):
+        chosen = mine(unit)
+
+        @pl.when(chosen[0])
+        def _():
+            slot = 2 * unit // parts
+            run([(slot, wave, 2 * unit, True) for wave in waves])
+
+        @pl.when(chosen[1])
+        def _():
+            slot = (2 * unit + 1) // parts
+            run(
+                [(slot, wave, 2 * unit, False) for wave in waves]
+                + [(slot, wave, 2 * unit + 1, True) for wave in waves]
+            )
+
+    def across_units(unit, other, waves):
+        query = jnp.maximum(unit, other)
+        key = jnp.minimum(unit, other)
+
+        def both(slot):
+            run([(slot, wave, 2 * key + side, False) for side in range(2) for wave in waves])
+
+        if parts == 2:
+            both(query)
+        else:
+            chosen = mine(query)
+            for side in range(2):
+                pl.when(chosen[side])(functools.partial(both, (2 * query + side) // parts))
+
+    def settle(unit):
+        for side in range(2):
+            arrive(2 * unit + side)
+
+    def visit(rank, unused):
+        unit = visit_unit(rank)
+        settle(unit)
+        pl.when(rank == 1)(lambda: forward("second"))
+        within(unit, (0, 1))
 
         def earlier(other_rank, unused):
-            other = visit_place(other_rank)
-            query = jnp.maximum(origin, other)
-            key = jnp.minimum(origin, other)
-
-            @pl.when(owner_of(query) == my_part)
-            def _():
-                block(query // parts, key, False)
-
+            across_units(unit, visit_unit(other_rank), (0, 1))
             return unused
 
         lax.fori_loop(0, rank, earlier, 0)
-        pl.when((z > 0) & (rank == 2 * z - 1))(chain)
+        pl.when(rank == 0)(lambda: forward("first"))
+        pl.when(rank == 1)(lambda: forward("seconded"))
+        pl.when(rank == z)(chain)
         return unused
-
-    lax.fori_loop(0, spans, visit, 0)
 
     eye = lax.broadcasted_iota(jnp.int32, (HEAD, HEAD), 0) == lax.broadcasted_iota(
         jnp.int32, (HEAD, HEAD), 1
@@ -527,29 +587,56 @@
     def span_of(slot):
         return slot * parts + (my_part if slot % 2 == 0 else parts - 1 - my_part)
 
-    def att_copy(slot):
+    def att_place(wave):
+        return attended_ref.at[wave, pl.ds(pl.multiple_of(my_head * HEAD, HEAD), HEAD)]
+
+    def att_copy(slot, wave):
         return remote(
-            att_out.at[slot], attended_ref.at[pl.ds(pl.multiple_of(my_head * HEAD, HEAD), HEAD)],
-            att_send.at[slot], att_recv.at[my_head], "sp", span_of(slot),
+            att_out.at[slot, wave], att_place(wave), att_send.at[slot, wave],
+            att_recv.at[my_head, wave], "sp", span_of(slot),
         )
 
-    for slot in range(heads):
-        first, second = (
-            acc_ref[slot, :HEAD, half * rows : (half + 1) * rows]
-            / acc_ref[slot, HEAD : HEAD + 1, half * rows : (half + 1) * rows]
-            for half in range(2)
-        )
-        difference = first - factor_second * second
-        mean = jnp.mean(difference * difference, axis=0, keepdims=True)
-        att_out[slot] = (difference * lax.rsqrt(mean + EPSILON) * head_gain).astype(jnp.bfloat16)
-
-        @pl.when(span_of(slot) == me)
-        def _():
-            attended_ref[pl.ds(pl.multiple_of(my_head * HEAD, HEAD), HEAD), :] = att_out[slot]
-
-        @pl.when(span_of(slot) != me)
-        def _():
-            att_copy(slot).start()
+    def finish(wave):
+        for slot in range(heads):
+            sums = acc_ref[slot, wave]
+            maps = sums[:HEAD] / sums[HEAD : HEAD + 1]
+            second = pltpu.roll(maps, half_rows, 1)[:, :half_rows]
+            difference = maps[:, :half_rows] - factor_second * second
+            mean = jnp.mean(difference * difference, axis=0, keepdims=True)
+            att_out[slot, wave] = (
+                difference * lax.rsqrt(mean + EPSILON) * head_gain
+            ).astype(jnp.bfloat16)
+
+            @pl.when(span_of(slot) == me)
+            def _():
+                att_place(wave)[...] = att_out[slot, wave]
+
+            @pl.when(span_of(slot) != me)
+            def _():
+                att_copy(slot, wave).start()
+
+    lax.fori_loop(0, units - 1, visit, 0)
+    last = visit_unit(units - 1)
+    settle(last)
+    for wave in range(2):
+        within(last, (wave,))
+        if parts == 2:
+            steps = []
+            for rank in range(units - 1):
+                other = visit_unit(rank)
+                query = jnp.maximum(last, other)
+                key = jnp.minimum(last, other)
+                steps.append([(query, wave, 2 * key + side, False) for side in range(2)])
+            run([step for side in zip(*steps) for step in side])
+        else:
+
+            def earlier(rank, unused):
+                across_units(last, visit_unit(rank), (wave,))
+                return unused
+
+            lax.fori_loop(0, units - 1, earlier, 0)
+        finish(wave)
+    pl.when(z == units - 1)(chain)
 
     stable = enter_ref[HEAD + 1 : HEAD + 2, :]
     memory_in = enter_ref[:HEAD, :]
@@ -583,15 +670,10 @@
 
     loads[6].wait()
     loads[7].wait()
-    for step in range(heads):
-        here = (my_owner != my_part) | (my_head != step)
-
-        @pl.when(here)
-        def _():
-            at = attended_ref.at[pl.ds(step * HEAD, HEAD)]
-            remote(at, at, att_send.at[0], att_recv.at[step], "sp", me).wait_recv()
+    partial_ref[...] = dot(memory_ref[...], som[...])
 
     out_span = rows // out_chunks
+    per_wave = out_chunks // 2
 
     def out_rows(chunk):
         return pl.ds(chunk * out_span, out_span)
@@ -618,23 +700,30 @@
             copy.start()
             lined[step, chunk] = copy
 
-    for chunk in range(out_chunks):
-        at = slice(chunk * out_span, (chunk + 1) * out_span)
+    for wave in range(2):
+        for step in range(heads):
+
+            @pl.when((my_owner != my_part) | (my_head != step))
+            def _():
+                at = attended_ref.at[wave, pl.ds(step * HEAD, HEAD)]
+                remote(at, at, att_send.at[0, wave], att_recv.at[step, wave], "sp", me).wait_recv()
+
+        at = slice(wave * half_rows, (wave + 1) * half_rows)
         part_ref[at, :] = (
-            dot(attended_ref[:, at], soa[...], ((0,), (0,))) + dot(memory_ref[at, :], som[...])
+            dot(attended_ref[wave], soa[...], ((0,), (0,))) + partial_ref[at, :]
         ).astype(jnp.bfloat16)
-        for step in order:
-            target = lax.rem(line + step, lines) * CORES + (1 - core)
-            copy = remote(
-                part_ref.at[out_rows(chunk), columns_of(target)],
-                pair_in.at[step, out_rows(chunk)], sp_send.at[step, chunk],
-                sp_recv.at[step, chunk], "tp", pair,
-            )
-            copy.start()
-            swaps[step, chunk] = copy
-        if chunk > 0:
-            pass_on(chunk - 1)
-    pass_on(out_chunks - 1)
+        for chunk in range(wave * per_wave, (wave + 1) * per_wave):
+            for step in order:
+                target = lax.rem(line + step, lines) * CORES + (1 - core)
+                copy = remote(
+                    part_ref.at[out_rows(chunk), columns_of(target)],
+                    pair_in.at[step, out_rows(chunk)], sp_send.at[step, chunk],
+                    sp_recv.at[step, chunk], "tp", pair,
+                )
+                copy.start()
+                swaps[step, chunk] = copy
+        for chunk in range(wave * per_wave, (wave + 1) * per_wave):
+            pass_on(chunk)
 
     for copy in sends:
         copy.wait_send()
@@ -660,7 +749,8 @@
 
         @pl.when(span_of(slot) != me)
         def _():
-            att_copy(slot).wait_send()
+            for wave in range(2):
+                att_copy(slot, wave).wait_send()
 
     for chunk in range(out_chunks):
         total = pair_sum(0, chunk)
@@ -686,7 +776,7 @@
     spans = depth * across
     parts = spans // heads
     chunks = 4
-    out_chunks = 3
+    out_chunks = 4
     dma = pltpu.SemaphoreType.DMA
 
     middle = DD // 2
@@ -704,26 +794,28 @@
         out_shape=jax.ShapeDtypeStruct((rows, columns), jnp.bfloat16),
         in_specs=[VMEM] * 4 + [hbm] * 6 + [VMEM] * 6 + [hbm] * 2,
         out_specs=VMEM,
-        scratch_shapes=[bf16(features, width)] * 6
+        scratch_shapes=[bf16(features, 6 * width)]
         + [bf16(width, features)] * 2
         + [
             bf16(rows, features), bf16(rows, features), f32(rows, 1), f32(rows, 6 * width),
             f32(rows, 128), f32(rows, 128),
             bf16(heads, rows, 128), bf16(heads, rows // 2, 128), bf16(spans, rows, 128),
             bf16(heads, rows // 2, 128), bf16(spans, VALUE_ROWS, rows),
-            bf16(heads, 2 * rows, 128), f32(heads, 1, 2 * rows), f32(heads, VALUE_ROWS, 2 * rows),
-            bf16(heads, HEAD, rows), bf16(width, rows),
+            bf16(2, rows, 128), bf16(heads, 2, 128, rows), f32(heads, 2, 1, rows),
+            f32(heads, 2, VALUE_ROWS, rows), bf16(heads, 2, HEAD, rows // 2),
+            bf16(2, width, rows // 2),
             bf16(rows, width), bf16(rows, width), bf16(rows, width), f32(rows, 128),
             f32(across, STATE_ROWS, width), f32(STATE_ROWS, width), f32(STATE_ROWS, width),
             f32(STATE_ROWS, width),
             f32(rows, width), f32(rows, 128), f32(rows, 128), f32(rows, 128), f32(8, rows),
             bf16(rows, width),
-            bf16(rows, features), bf16(lines, rows, columns), bf16(lines, rows, columns),
+            f32(rows, features), bf16(rows, features), bf16(lines, rows, columns),
+            bf16(lines, rows, columns),
             bf16(lines, rows, columns),
             dma((8,)), dma((lines, chunks)), dma((lines, chunks)), dma((lines, chunks)),
             dma((lines, chunks)),
             dma((heads, chunks)), dma((heads, parts, chunks)), dma((spans, chunks)),
-            dma((heads, chunks)), dma((heads, chunks)), dma((heads,)), dma((heads,)),
+            dma((heads, chunks)), dma((heads, chunks)), dma((heads, 2)), dma((heads, 2)),
             dma((across,)), dma((across,)), dma(()), dma(()),
             dma((lines, out_chunks)), dma((lines, out_chunks)), dma((lines, out_chunks)),
             dma((lines, out_chunks)),

time: 69.8 us -> 59.4 us (0.85)
  Pallas kernels: 67 us -> 56.6 us
    pallas_call x1, Pallas kernels: 67 us -> 56.6 us  [per_device(): pl.pallas_call(functools.partial(layer_kernel, tp_size, depth, across, ch...]
where the time goes in v2:
time: 59.4 us; the launch traced here: 59.2 us
  Pallas kernels  56.6 us (95%)
  local copies, waits for them, and re-layouts  1.77 us (3%)
  other arithmetic  0.82 us (1%)
    pallas_call x1, Pallas kernels, per_device(): pl.pallas_call(functools.partial(layer_kernel, tp_size, depth, across, ch...  56.6 us
    unnamed x1, local copies, waits for them, and re-layouts  1.77 us

profile of v2, /device:TPU:0, one launch (start us, length us, event | category | flops | bytes accessed | tf_op | source)
XLA Modules:
  0.0 59.2 jit_solution(5670745958986909593)
XLA Ops:
  0.0 0.8 %multiply_sine_fusion = (f32[16,384]{1,0:T(8,128)}, f32[16,384]{1,0:T(8,128)}) fusion(f32[384]{0:T(512)S(1)} %add_convert_fusion, f32[16]{0:T(128)S(1)} %negate_power_fusion), kind=kLoop, calls=%fused_computation | loop fusion | flops 6144 | bytes 50752 | tf_op jit(solution)/shard_map/sin | solution.py:787
  0.8 56.6 %layer.1 = bf16[384,512]{1,0:T(8,128)(2,1)} custom-call(bf16[384,512]{1,0:T(8,128)(2,1)} %shard_ref.1, f32[1,2048]{1,0:T(1,128)} %bitcast.9, f32[16,384]{1,0:T(8,128)} %get-tuple-element.6.cos_ref, f32[16,384]{1,0:T(8,128)} %get-tuple-element.5.sin_ref, bf16[2048,256]{1,0:T(8,128)(2,1)} %wq.1, bf16[2048,256]{1,0:T(8,128)(2,1)} %wk.1, bf16[2048,256]{1,0:T(8,128)(2,1)} %wv.1, ...), custom_call_target="tpu_custom_call" | custom-call | tf_op jit(solution)/shard_map/layer/pallas_call | solution.py:792
  57.4 1.8 %copy.18 = bf16[384,512]{1,0:T(8,128)(2,1)} copy(bf16[384,512]{1,0:T(8,128)(2,1)} %layer.1) | data formatting | bytes 786432
  (2 shorter events, 0.0 us)

commit v3 on v2

--- a/solution.py
+++ b/solution.py
@@ -61,14 +61,16 @@
 def near_first(place, count, rank):
     both = jnp.minimum(place, count - 1 - place)
     half = (rank + 1) // 2
-    alternating = jnp.where(rank % 2 == 1, place - half, place + half)
-    one_sided = jnp.where(place < count - 1 - place, rank, count - 1 - rank)
+    low = place < count - 1 - place
+    below = jnp.where(low, rank % 2 == 1, rank % 2 == 0)
+    alternating = jnp.where(below, place - half, place + half)
+    one_sided = jnp.where(low, rank, count - 1 - rank)
     return jnp.where(rank <= 2 * both, alternating, one_sided)
 
 
 def layer_kernel(
     size, depth, across, chunks, out_chunks,
-    shard_ref, gain_ref, cos_ref, sin_ref, wq, wk, wv, wmq, wmk, wmv, wi, wf, bias_ref, shift_ref,
+    shard_ref, gain_ref, rate_ref, wq, wk, wv, wmq, wmk, wmv, wi, wf, bias_ref, shift_ref,
     lambda_ref, head_gain_ref, woa, wom,
     out_ref,
     weight_ref, soa, som, x_ref, scaled_ref, square_ref, sum_ref, cosine_ref, sine_ref,
@@ -125,8 +127,12 @@
     for step in range(1, spans):
         signal(barrier, "sp", lax.rem(me + step, spans))
 
-    cosine_ref[...] = jnp.concatenate([cos_ref[...]] * (128 * 2 // DD), axis=0).T
-    sine_ref[...] = jnp.concatenate([-sin_ref[...], sin_ref[...]] * (128 // DD), axis=0).T
+    position = (me * rows + lax.broadcasted_iota(jnp.int32, (1, rows), 1)).astype(jnp.float32)
+    angles = rate_ref[...] * position
+    cosines = jnp.cos(angles)
+    sines = jnp.sin(angles)
+    cosine_ref[...] = jnp.concatenate([cosines] * (128 * 2 // DD), axis=0).T
+    sine_ref[...] = jnp.concatenate([-sines, sines] * (128 // DD), axis=0).T
     lanes = lax.broadcasted_iota(jnp.int32, (1, 128), 1)
     former = lax.rem(lanes, DD) < DD // 2
     low_lanes = lanes < HEAD
@@ -192,7 +198,7 @@
         return wide * cosine + partner * sine
 
     def kv_sends(chunk):
-        for rank in range(heads - 1, 0, -1):
+        for rank in range(1, heads):
             head = near_first(my_head, heads, rank)
             yield remote(
                 kv_out.at[head, rows_of(chunk)], kv_all.at[me, rows_of(chunk)],
@@ -208,9 +214,9 @@
             )
 
     points = {
-        (1, 0): "chunk2", (2, 0): "projected", (3, 0): "projected", (1, 1): "projected",
-        (2, 1): "state", (1, 2): "state", (3, 1): "inner", (2, 2): "inner", (1, 3): "inner",
-        (3, 2): "first", (2, 3): "second", (3, 3): "seconded",
+        (1, 0): "chunk1", (1, 1): "chunk2", (1, 2): "projected", (2, 0): "projected",
+        (1, 3): "state", (3, 0): "state", (2, 1): "first", (3, 1): "first",
+        (2, 2): "inner", (3, 2): "second", (2, 3): "second", (3, 3): "seconded",
     }
 
     def landed(rank):
@@ -233,7 +239,7 @@
     my_owner = owner_of(me)
 
     def q_sends(chunk):
-        for rank in range(heads - 1, 0, -1):
+        for rank in range(1, heads):
             head = near_first(my_head, heads, rank)
             yield remote(
                 q_out.at[head, packed_of(chunk)], q_all.at[my_slot, packed_of(chunk)],
@@ -246,20 +252,22 @@
             q_send.at[0, chunk], q_recv.at[my_slot, chunk], "sp", my_head * parts + my_owner,
         )
 
+    def pull(chunk):
+        for step in range(1, lines):
+            source = lax.rem(line + lines - step, lines) * CORES + core
+            at = place(source, chunk)
+            remote(
+                at, at, line_send.at[step, chunk], line_recv.at[step, chunk], "tp", pair
+            ).wait_recv()
+            copy = remote(
+                at, at, pair_send.at[step, chunk], pair_recv.at[step, chunk], "tp", pair
+            )
+            copy.start()
+            pairs[step, chunk] = copy
+
+    pull(0)
     for chunk in range(chunks):
         at = rows_of(chunk)
-        for step in range(1, lines):
-            source = lax.rem(line + lines - step, lines) * CORES + core
-            remote(
-                place(source, chunk), place(source, chunk), line_send.at[step, chunk],
-                line_recv.at[step, chunk], "tp", pair,
-            ).wait_recv()
-            copy = remote(
-                place(source, chunk), place(source, chunk), pair_send.at[step, chunk],
-                pair_recv.at[step, chunk], "tp", pair,
-            )
-            copy.start()
-            pairs[step, chunk] = copy
         squares = square_ref[at]
         for step in range(1, lines):
             source = lax.rem(line + lines - step, lines) * CORES + core
@@ -319,6 +327,8 @@
             q_aside(chunk).start()
 
         mk_ref[at] = memory_keys.astype(jnp.bfloat16)
+        if chunk + 1 < chunks:
+            pull(chunk + 1)
         memory_values, memory_queries = products(2)
         mv_ref[at] = memory_values.astype(jnp.bfloat16)
         mq_ref[at] = memory_queries.astype(jnp.bfloat16)
@@ -341,7 +351,8 @@
     lower_ones = lower.astype(jnp.bfloat16)
     first, rest = two_parts(forget)
     second = (forget - first.astype(jnp.float32) - rest.astype(jnp.float32)).astype(jnp.bfloat16)
-    cumulative = dot(lower_ones, first) + (dot(lower_ones, rest) + dot(lower_ones, second))
+    sums = dot(lower_ones, jnp.concatenate([first, rest, second], axis=1))
+    cumulative = sums[:, :heads] + (sums[:, heads : 2 * heads] + sums[:, 2 * heads :])
     cumulative_ref[:, :heads] = cumulative
     offsets = jnp.concatenate(
         [gate - cumulative, jnp.zeros((rows, 128 - heads), jnp.float32)], axis=1
@@ -372,33 +383,40 @@
                 z * across + lax.rem(x + step, across),
             )
 
+    forward("state")
     for copy in state_sends():
         copy.start()
 
-    forward("state")
-    for group in range(groups):
-        lane_group = slice(group * 128, (group + 1) * 128)
-        keys = mk_ref[:, lane_group]
-        values = mv_ref[:, lane_group]
-        group_queries = mq_ref[:, lane_group]
-        result = None
-        for side in range(2):
-            head = group * 2 + side
-            chosen = (lanes // HEAD) == side
-            column = cumulative[:, head : head + 1]
-            gaps = jnp.where(lower, column + offset_ref[head : head + 1, :], NEGATIVE)
-            row_top = jnp.max(gaps, axis=1, keepdims=True)
-            within = jnp.exp(gaps - row_top)
-            scores = dot(jnp.where(chosen, group_queries, 0), keys, ((1,), (1,)))
-            scores = jnp.where(lower, within * (scores * (HEAD**-0.5)), 0.0)
-            inner_den[:, head : head + 1] = jnp.sum(scores, axis=1, keepdims=True)
-            inner_top[:, head : head + 1] = row_top
-            score_high, score_low = two_parts(scores)
-            numerator = dot(score_high, values) + dot(score_low, values)
-            result = numerator if result is None else jnp.where(chosen, numerator, result)
-        inner_ref[:, lane_group] = result
-
-    forward("inner")
+    def inner():
+        step_rows = 128
+        for group in range(groups):
+            lane_group = slice(group * 128, (group + 1) * 128)
+            for start in range(0, rows, step_rows):
+                stop = start + step_rows
+                block_rows = slice(start, stop)
+                keys = mk_ref[:stop, lane_group]
+                values = mv_ref[:stop, lane_group]
+                group_queries = mq_ref[block_rows, lane_group]
+                row_index = lax.broadcasted_iota(jnp.int32, (step_rows, stop), 0)
+                column_index = lax.broadcasted_iota(jnp.int32, (step_rows, stop), 1)
+                lower = column_index <= row_index + start
+                result = None
+                for side in range(2):
+                    head = group * 2 + side
+                    chosen = (lanes // HEAD) == side
+                    column = cumulative_ref[block_rows, head : head + 1]
+                    gaps = jnp.where(lower, column + offset_ref[head : head + 1, :stop], NEGATIVE)
+                    row_top = jnp.max(gaps, axis=1, keepdims=True)
+                    within = jnp.exp(gaps - row_top)
+                    scores = dot(jnp.where(chosen, group_queries, 0), keys, ((1,), (1,)))
+                    scores = jnp.where(lower, within * (scores * (HEAD**-0.5)), 0.0)
+                    inner_den[block_rows, head : head + 1] = jnp.sum(scores, axis=1, keepdims=True)
+                    inner_top[block_rows, head : head + 1] = row_top
+                    score_high, score_low = two_parts(scores)
+                    numerator = dot(score_high, values) + dot(score_low, values)
+                    result = numerator if result is None else jnp.where(chosen, numerator, result)
+                inner_ref[block_rows, lane_group] = result
+
     def advance(body, stable, later):
         later_top = later[HEAD + 1 : HEAD + 2, :]
         decay = later[HEAD + 2 : HEAD + 3, :]
@@ -563,6 +581,7 @@
         unit = visit_unit(rank)
         settle(unit)
         pl.when(rank == 1)(lambda: forward("second"))
+        pl.when((z > 0) & (rank == z + 1))(chain)
         within(unit, (0, 1))
 
         def earlier(other_rank, unused):
@@ -570,9 +589,7 @@
             return unused
 
         lax.fori_loop(0, rank, earlier, 0)
-        pl.when(rank == 0)(lambda: forward("first"))
         pl.when(rank == 1)(lambda: forward("seconded"))
-        pl.when(rank == z)(chain)
         return unused
 
     eye = lax.broadcasted_iota(jnp.int32, (HEAD, HEAD), 0) == lax.broadcasted_iota(
@@ -615,9 +632,51 @@
             def _():
                 att_copy(slot, wave).start()
 
-    lax.fori_loop(0, units - 1, visit, 0)
+    def recall():
+        stable = enter_ref[HEAD + 1 : HEAD + 2, :]
+        memory_in = enter_ref[:HEAD, :]
+        normal_in = enter_ref[HEAD : HEAD + 1, :]
+        blocks = jnp.concatenate(
+            [jnp.where(head_mask(width, head), memory_in, 0.0) for head in range(heads)], axis=0
+        )
+        high, low = two_parts(blocks)
+        memory_queries = mq_ref[...]
+        carried_part = dot(memory_queries, high) + dot(memory_queries, low)
+        weighted = memory_queries.astype(jnp.float32) * normal_in
+        for group in range(groups):
+            lane_group = slice(group * 128, (group + 1) * 128)
+            result = None
+            for side in range(2):
+                head = group * 2 + side
+                chosen = (lanes // HEAD) == side
+                column = slice(head, head + 1)
+                carried_log = cumulative_ref[:, column] + stable[:, head * HEAD : head * HEAD + 1]
+                own_top = inner_top[:, column]
+                row_top = jnp.maximum(carried_log, own_top)
+                inside = jnp.exp(own_top - row_top)
+                outside = jnp.exp(carried_log - row_top)
+                denominator = inside * inner_den[:, column] + outside * jnp.sum(
+                    jnp.where(chosen, weighted[:, lane_group], 0.0), axis=1, keepdims=True
+                )
+                numerator = inside * inner_ref[:, lane_group] + outside * carried_part[:, lane_group]
+                quotient = numerator / jnp.maximum(jnp.abs(denominator), 1.0)
+                result = quotient if result is None else jnp.where(chosen, quotient, result)
+            memory_ref[:, lane_group] = result.astype(jnp.bfloat16)
+
+        loads[6].wait()
+        loads[7].wait()
+        partial_ref[...] = dot(memory_ref[...], som[...])
+
+    settle(me // 2)
+    within(me // 2, (0, 1))
+    forward("first")
+    inner()
+    forward("inner")
+    pl.when(z == 0)(chain)
+    lax.fori_loop(1, units - 1, visit, 0)
     last = visit_unit(units - 1)
     settle(last)
+    pl.when(z == units - 2)(chain)
     for wave in range(2):
         within(last, (wave,))
         if parts == 2:
@@ -636,41 +695,12 @@
 
             lax.fori_loop(0, units - 1, earlier, 0)
         finish(wave)
-    pl.when(z == units - 1)(chain)
-
-    stable = enter_ref[HEAD + 1 : HEAD + 2, :]
-    memory_in = enter_ref[:HEAD, :]
-    normal_in = enter_ref[HEAD : HEAD + 1, :]
-    blocks = jnp.concatenate(
-        [jnp.where(head_mask(width, head), memory_in, 0.0) for head in range(heads)], axis=0
-    )
-    high, low = two_parts(blocks)
-    memory_queries = mq_ref[...]
-    carried_part = dot(memory_queries, high) + dot(memory_queries, low)
-    weighted = memory_queries.astype(jnp.float32) * normal_in
-    for group in range(groups):
-        lane_group = slice(group * 128, (group + 1) * 128)
-        result = None
-        for side in range(2):
-            head = group * 2 + side
-            chosen = (lanes // HEAD) == side
-            column = slice(head, head + 1)
-            carried_log = cumulative_ref[:, column] + stable[:, head * HEAD : head * HEAD + 1]
-            own_top = inner_top[:, column]
-            row_top = jnp.maximum(carried_log, own_top)
-            inside = jnp.exp(own_top - row_top)
-            outside = jnp.exp(carried_log - row_top)
-            denominator = inside * inner_den[:, column] + outside * jnp.sum(
-                jnp.where(chosen, weighted[:, lane_group], 0.0), axis=1, keepdims=True
-            )
-            numerator = inside * inner_ref[:, lane_group] + outside * carried_part[:, lane_group]
-            quotient = numerator / jnp.maximum(jnp.abs(denominator), 1.0)
-            result = quotient if result is None else jnp.where(chosen, quotient, result)
-        memory_ref[:, lane_group] = result.astype(jnp.bfloat16)
-
-    loads[6].wait()
-    loads[7].wait()
-    partial_ref[...] = dot(memory_ref[...], som[...])
+        if wave == 0:
+            pl.when(z < units - 1)(recall)
+    @pl.when(z >= units - 1)
+    def _():
+        chain()
+        recall()
 
     out_span = rows // out_chunks
     per_wave = out_chunks // 2
@@ -781,10 +811,6 @@
 
     middle = DD // 2
     inverse = 1.0 / ROTARY_BASE ** (jnp.arange(middle, dtype=jnp.float32) / middle)
-    positions = lax.axis_index("sp") * rows + jnp.arange(rows, dtype=jnp.int32)
-    angles = inverse[:, None] * positions.astype(jnp.float32)[None, :]
-    cosine = jnp.cos(angles)
-    sine = jnp.sin(angles)
 
     hbm = pl.BlockSpec(memory_space=pl.ANY)
     bf16 = lambda *shape: pltpu.VMEM(shape, jnp.bfloat16)
@@ -792,7 +818,7 @@
     return pl.pallas_call(
         functools.partial(layer_kernel, tp_size, depth, across, chunks, out_chunks),
         out_shape=jax.ShapeDtypeStruct((rows, columns), jnp.bfloat16),
-        in_specs=[VMEM] * 4 + [hbm] * 6 + [VMEM] * 6 + [hbm] * 2,
+        in_specs=[VMEM] * 3 + [hbm] * 6 + [VMEM] * 6 + [hbm] * 2,
         out_specs=VMEM,
         scratch_shapes=[bf16(features, 6 * width)]
         + [bf16(width, features)] * 2
@@ -825,7 +851,7 @@
         ),
         name="layer",
     )(
-        inputs, norm_gain[None, :], cosine, sine, query_weight, key_weight, value_weight,
+        inputs, norm_gain[None, :], inverse[:, None], query_weight, key_weight, value_weight,
         memory_query_weight, memory_key_weight, memory_value_weight, input_gate_weight.T,
         forget_gate_weight.T, forget_bias[None, :], decay_shift.T, lambdas[None, :],
         head_gain[None, :], out_weight_attention, out_weight_memory,

time: 59.4 us -> 56.4 us (0.949)
  Pallas kernels: 56.6 us -> 53.9 us
    pallas_call x1, Pallas kernels: 56.6 us -> 53.9 us  [per_device(): pl.pallas_call(functools.partial(layer_kernel, tp_size, depth, across, ch...]
    sin x1 -> x0, other arithmetic: 0.81 us -> none  [per_device(): sine = jnp.sin(angles)]
    pow x1, other arithmetic: 0.01 us -> 0.61 us  [per_device(): ROTARY_BASE ** (jnp.arange(middle, dtype=jnp.float32) / middle)]
where the time goes in v3:
time: 56.4 us; the launch traced here: 56.3 us
  Pallas kernels  53.9 us (96%)
  local copies, waits for them, and re-layouts  1.77 us (3%)
  other arithmetic  0.61 us (1%)
    pallas_call x1, Pallas kernels, per_device(): pl.pallas_call(functools.partial(layer_kernel, tp_size, depth, across, ch...  53.9 us
    unnamed x1, local copies, waits for them, and re-layouts  1.77 us

profile of v3, /device:TPU:0, one launch (start us, length us, event | category | flops | bytes accessed | tf_op | source)
XLA Modules:
  0.0 56.3 jit_solution(12823297491098346639)
XLA Ops:
  0.0 0.6 %negate_power_fusion.rate_ref = f32[16,1]{1,0:T(8,128)} fusion(), kind=kLoop, calls=%fused_computation | loop fusion | flops 32 | bytes 64 | tf_op jit(solution)/shard_map/pow | solution.py:813
  0.6 53.9 %layer.1 = bf16[384,512]{1,0:T(8,128)(2,1)} custom-call(bf16[384,512]{1,0:T(8,128)(2,1)} %shard_ref.1, f32[1,2048]{1,0:T(1,128)} %bitcast.9, f32[16,1]{1,0:T(8,128)} %negate_power_fusion.rate_ref, bf16[2048,256]{1,0:T(8,128)(2,1)} %wq.1, bf16[2048,256]{1,0:T(8,128)(2,1)} %wk.1, bf16[2048,256]{1,0:T(8,128)(2,1)} %wv.1, bf16[2048,256]{1,0:T(8,128)(2,1)} %wmq.1, ...), custom_call_target="tpu_custom_call" | custom-call | tf_op jit(solution)/shard_map/layer/pallas_call | solution.py:818
  54.5 1.8 %copy.18 = bf16[384,512]{1,0:T(8,128)(2,1)} copy(bf16[384,512]{1,0:T(8,128)(2,1)} %layer.1) | data formatting | bytes 786432

commit v4 on v3

--- a/solution.py
+++ b/solution.py
@@ -41,14 +41,6 @@
     return (lanes // HEAD) == head
 
 
-def spread(columns, width):
-    spreaded = columns[:, 0:1]
-    for head in range(1, columns.shape[1]):
-        lanes = lax.broadcasted_iota(jnp.int32, (1, width), 1)
-        spreaded = jnp.where(lanes >= head * HEAD, columns[:, head : head + 1], spreaded)
-    return jnp.broadcast_to(spreaded, (columns.shape[0], width))
-
-
 def two_parts(floats):
     high = floats.astype(jnp.bfloat16)
     return high, (floats - high.astype(jnp.float32)).astype(jnp.bfloat16)
@@ -70,18 +62,17 @@
 
 def layer_kernel(
     size, depth, across, chunks, out_chunks,
-    shard_ref, gain_ref, rate_ref, wq, wk, wv, wmq, wmk, wmv, wi, wf, bias_ref, shift_ref,
+    shard_ref, gain_ref, wq, wk, wv, wmq, wmk, wmv, wi, wf, bias_ref, shift_ref,
     lambda_ref, head_gain_ref, woa, wom,
     out_ref,
     weight_ref, soa, som, x_ref, scaled_ref, square_ref, sum_ref, cosine_ref, sine_ref,
     kv_out, q_out, kv_all, q_all, vt_ref, qn_ref, qt_ref, top_ref, acc_ref, att_out, attended_ref,
-    mq_ref, mk_ref, mv_ref, pre_ref, states_ref, prefix_in, prefix_out, enter_ref,
+    mq_ref, mk_ref, mv_ref, mq_turned, mv_turned, pre_ref, states_ref, prefix_in, prefix_out, enter_ref,
     inner_ref, inner_den, inner_top, cumulative_ref, offset_ref, memory_ref,
-    partial_ref, part_ref, pair_in, line_out, line_in,
-    load_sems, line_send, line_recv, pair_send, pair_recv,
-    kv_send, fwd_send, kv_recv, q_send, q_recv, att_send, att_recv,
-    st_send, st_recv, px_send, px_recv,
-    sp_send, sp_recv, sl_send, sl_recv,
+    partial_ref, part_ref, pair_in, line_out, line_in, total_ref,
+    out_sem, load_sems, line_send, line_recv, pair_send, pair_recv, own_recv,
+    kv_send, fwd_send, land_recv, cross_recv, q_send, q_side, q_recv, att_send, att_recv,
+    st_send, st_recv, px_send, px_recv, sp_send, sp_recv, sl_send, sl_recv,
 ):
     rows, columns = shard_ref.shape
     features = x_ref.shape[1]
@@ -128,7 +119,12 @@
         signal(barrier, "sp", lax.rem(me + step, spans))
 
     position = (me * rows + lax.broadcasted_iota(jnp.int32, (1, rows), 1)).astype(jnp.float32)
-    angles = rate_ref[...] * position
+    middle = DD // 2
+    turn = lax.broadcasted_iota(jnp.int32, (middle, 1), 0)
+    rates = jnp.zeros((middle, 1), jnp.float32)
+    for index in range(middle):
+        rates = jnp.where(turn == index, ROTARY_BASE ** (-index / middle), rates)
+    angles = rates * position
     cosines = jnp.cos(angles)
     sines = jnp.sin(angles)
     cosine_ref[...] = jnp.concatenate([cosines] * (128 * 2 // DD), axis=0).T
@@ -148,23 +144,16 @@
 
     pl.semaphore_wait(barrier, lines + spans - 1)
 
-    sends = []
     pairs = {}
     for chunk in range(chunks):
         for step in range(1, lines):
             copy = remote(
-                shard_ref.at[rows_of(chunk)], place(tp, chunk), line_send.at[step, chunk],
-                line_recv.at[step, chunk], "tp", lax.rem(line + step, lines) * CORES + core,
+                shard_ref.at[rows_of(chunk)], place(tp, chunk), line_send,
+                line_recv.at[step - 1, chunk], "tp", lax.rem(line + step, lines) * CORES + core,
             )
             copy.start()
-            sends.append(copy)
-    for chunk in range(chunks):
-        copy = remote(
-            shard_ref.at[rows_of(chunk)], place(tp, chunk), pair_send.at[0, chunk],
-            pair_recv.at[0, chunk], "tp", pair,
-        )
-        copy.start()
-        pairs[0, chunk] = copy
+    own_pair = remote(shard_ref, x_ref.at[:, columns_of(tp)], pair_send, own_recv, "tp", pair)
+    own_pair.start()
 
     def take(values, at_rows, owner):
         floats = values.astype(jnp.float32)
@@ -175,8 +164,7 @@
 
     everywhere = pl.ds(0, rows)
     squares = take(shard_ref[...], everywhere, tp)
-    for chunk in range(chunks):
-        pairs[0, chunk].wait_recv()
+    own_pair.wait_recv()
     square_ref[...] = squares + take(x_ref[:, columns_of(pair)], everywhere, pair)
 
     def line_columns(owner_line):
@@ -190,7 +178,14 @@
             scaled_ref[:, line_columns(line)], weight_ref[line_columns(line), couple]
         )
 
-    gate_weights = jnp.concatenate([wi[...], wf[...]], axis=0)
+    blank = jnp.zeros((8 - heads, features), jnp.float32)
+    gate_weights = jnp.concatenate(
+        [wi[...].astype(jnp.float32), blank, wf[...].astype(jnp.float32), blank], axis=0
+    ).astype(jnp.bfloat16)
+    gate_bias = jnp.concatenate(
+        [jnp.zeros((1, 8), jnp.float32), bias_ref[...], jnp.zeros((1, 8 - heads), jnp.float32)],
+        axis=1,
+    )
     factor = (DD**-0.5) * LOG2E
 
     def rotated(wide, cosine, sine):
@@ -202,36 +197,35 @@
             head = near_first(my_head, heads, rank)
             yield remote(
                 kv_out.at[head, rows_of(chunk)], kv_all.at[me, rows_of(chunk)],
-                kv_send.at[rank, chunk], kv_recv.at[me, chunk], "sp", head * parts + my_part,
-            )
-
-    def forwards(source, origin, index, chunk):
+                kv_send, land_recv.at[my_head, chunk], "sp", head * parts + my_part,
+            )
+
+    def forwards(source, origin, chunk):
         for step in range(1, parts):
             yield remote(
-                source, kv_all.at[origin, rows_of(chunk)], fwd_send.at[index, step, chunk],
-                kv_recv.at[origin, chunk], "sp",
+                source, kv_all.at[origin, rows_of(chunk)], fwd_send, cross_recv.at[origin], "sp",
                 my_head * parts + lax.rem(my_part + step, parts),
             )
 
     points = {
         (1, 0): "chunk1", (1, 1): "chunk2", (1, 2): "projected", (2, 0): "projected",
-        (1, 3): "state", (3, 0): "state", (2, 1): "first", (3, 1): "first",
-        (2, 2): "inner", (3, 2): "second", (2, 3): "second", (3, 3): "seconded",
+        (1, 3): "state", (3, 0): "first", (2, 1): "first", (3, 1): "inner",
+        (2, 2): "inner", (2, 3): "second", (3, 2): "seconded", (3, 3): "seconded",
     }
 
     def landed(rank):
         return near_first(my_head, heads, rank) * parts + my_part
 
     def forward(point, index=""):
-        for chunk in range(chunks):
-            for rank in range(1, heads):
+        for rank in range(1, heads):
+            for chunk in range(chunks):
                 if points.get((rank, chunk), "inner") == f"{point}{index}":
                     origin = landed(rank)
                     at = kv_all.at[origin, rows_of(chunk)]
                     remote(
-                        at, at, kv_send.at[0, chunk], kv_recv.at[origin, chunk], "sp", me
+                        at, at, kv_send, land_recv.at[origin // parts, chunk], "sp", me
                     ).wait_recv()
-                    for copy in forwards(at, origin, origin // parts, chunk):
+                    for copy in forwards(at, origin, chunk):
                         copy.start()
 
     packed_of = lambda chunk: pl.ds(chunk * packed, packed)
@@ -243,13 +237,13 @@
             head = near_first(my_head, heads, rank)
             yield remote(
                 q_out.at[head, packed_of(chunk)], q_all.at[my_slot, packed_of(chunk)],
-                q_send.at[rank, chunk], q_recv.at[my_slot, chunk], "sp", head * parts + my_owner,
+                q_send, q_recv.at[my_slot], "sp", head * parts + my_owner,
             )
 
     def q_aside(chunk):
         return remote(
             q_out.at[my_head, packed_of(chunk)], q_all.at[my_slot, packed_of(chunk)],
-            q_send.at[0, chunk], q_recv.at[my_slot, chunk], "sp", my_head * parts + my_owner,
+            q_side, q_recv.at[my_slot], "sp", my_head * parts + my_owner,
         )
 
     def pull(chunk):
@@ -257,11 +251,9 @@
             source = lax.rem(line + lines - step, lines) * CORES + core
             at = place(source, chunk)
             remote(
-                at, at, line_send.at[step, chunk], line_recv.at[step, chunk], "tp", pair
+                at, at, line_send, line_recv.at[step - 1, chunk], "tp", pair
             ).wait_recv()
-            copy = remote(
-                at, at, pair_send.at[step, chunk], pair_recv.at[step, chunk], "tp", pair
-            )
+            copy = remote(at, at, pair_send, pair_recv.at[step - 1, chunk], "tp", pair)
             copy.start()
             pairs[step, chunk] = copy
 
@@ -301,7 +293,7 @@
             ).astype(jnp.bfloat16)
         for copy in kv_sends(chunk):
             copy.start()
-        for copy in forwards(kv_out.at[my_head, at], me, my_head, chunk):
+        for copy in forwards(kv_out.at[my_head, at], me, chunk):
             copy.start()
         kv_all[me, at] = kv_out[my_head, at]
 
@@ -332,54 +324,64 @@
         memory_values, memory_queries = products(2)
         mv_ref[at] = memory_values.astype(jnp.bfloat16)
         mq_ref[at] = memory_queries.astype(jnp.bfloat16)
-        pre_ref[at, : 2 * heads] = dot(scaled_ref[at, :], gate_weights, ((1,), (1,))) * inverse
+        pre_ref[at, :16] = dot(scaled_ref[at, :], gate_weights, ((1,), (1,))) * inverse + gate_bias
         if chunk < chunks - 1:
             forward("chunk", chunk)
 
     forward("projected")
 
-    gate = pre_ref[:, :heads]
-    pre = pre_ref[:, heads : 2 * heads] + bias_ref[...]
-    shift = shift_ref[...]
-    shift = jnp.concatenate(
-        [shift, jnp.zeros((128 - shift.shape[0], rows), jnp.float32)], axis=0
-    ).T[:, : shift.shape[0]]
+    turned = pre_ref[...].T
+    gate = turned[:8]
+    pre = turned[8:16]
+    shift = jnp.concatenate([shift_ref[...], jnp.zeros((8 - heads, rows), jnp.float32)], axis=0)
     forget = jnp.minimum(pre, 0.0) - jnp.log1p(jnp.exp(-jnp.abs(pre))) + shift
+    first, rest = (part.astype(jnp.float32) for part in two_parts(forget))
+    pieces = jnp.concatenate([first, rest, forget - first - rest], axis=0).astype(jnp.bfloat16)
     row_index = lax.broadcasted_iota(jnp.int32, (rows, rows), 0)
     column_index = lax.broadcasted_iota(jnp.int32, (rows, rows), 1)
-    lower = column_index <= row_index
-    lower_ones = lower.astype(jnp.bfloat16)
-    first, rest = two_parts(forget)
-    second = (forget - first.astype(jnp.float32) - rest.astype(jnp.float32)).astype(jnp.bfloat16)
-    sums = dot(lower_ones, jnp.concatenate([first, rest, second], axis=1))
-    cumulative = sums[:, :heads] + (sums[:, heads : 2 * heads] + sums[:, 2 * heads :])
-    cumulative_ref[:, :heads] = cumulative
-    offsets = jnp.concatenate(
-        [gate - cumulative, jnp.zeros((rows, 128 - heads), jnp.float32)], axis=1
+    sums = dot(pieces, (row_index <= column_index).astype(jnp.bfloat16))
+    cumulative = sums[:8] + (sums[8:16] + sums[16:24])
+    cumulative_ref[...] = cumulative
+    offset = gate - cumulative
+    offset_ref[...] = jnp.concatenate([offset, jnp.zeros((120, rows), jnp.float32)], axis=0).T
+    end = cumulative[:, rows - 1 : rows]
+    toward = end + offset
+    top = jnp.max(toward, axis=1, keepdims=True)
+    end_weights = jnp.exp(toward - top) * (HEAD**-0.5)
+    mv_turned[...] = mv_ref[...].T
+    mq_turned[...] = mq_ref[...].T
+    weighted = jnp.concatenate(
+        [
+            mv_turned[head * HEAD : (head + 1) * HEAD, :].astype(jnp.float32)
+            * end_weights[head : head + 1, :]
+            for head in range(heads)
+        ]
+        + [end_weights, end_weights],
+        axis=0,
     )
-    offset_ref[...] = offsets.T[:8, :]
-    end = cumulative[rows - 1 : rows, :]
-    toward = end - cumulative + gate
-    top = jnp.max(toward, axis=0, keepdims=True)
-    end_weights = spread(jnp.exp(toward - top), width)
-    keyed = mk_ref[...].astype(jnp.float32) * (HEAD**-0.5) * end_weights
-    high, low = two_parts(keyed)
-    whole = dot(high, mv_ref[...], ((0,), (0,))) + dot(low, mv_ref[...], ((0,), (0,)))
+    high, low = two_parts(weighted)
+    whole = dot(high, mk_ref[...]) + dot(low, mk_ref[...])
     memory = jnp.zeros((HEAD, width), jnp.float32)
+    normal = jnp.zeros((1, width), jnp.float32)
+    top_row = jnp.zeros((1, width), jnp.float32)
+    end_row = jnp.zeros((1, width), jnp.float32)
     for head in range(heads):
-        memory = jnp.where(
-            head_mask(width, head), whole[head * HEAD : (head + 1) * HEAD, :], memory
-        )
+        chosen = head_mask(width, head)
+        at_head = slice(head, head + 1)
+        memory = jnp.where(chosen, whole[head * HEAD : (head + 1) * HEAD, :], memory)
+        normal = jnp.where(chosen, whole[width + head : width + head + 1, :], normal)
+        top_row = jnp.where(chosen, top[at_head], top_row)
+        end_row = jnp.where(chosen, end[at_head], end_row)
     states_ref[x, :HEAD, :] = memory
-    states_ref[x, HEAD : HEAD + 1, :] = jnp.sum(keyed, axis=0, keepdims=True)
-    states_ref[x, HEAD + 1 : HEAD + 2, :] = spread(top, width)
-    states_ref[x, HEAD + 2 : HEAD + 3, :] = spread(end, width)
+    states_ref[x, HEAD : HEAD + 1, :] = normal
+    states_ref[x, HEAD + 1 : HEAD + 2, :] = top_row
+    states_ref[x, HEAD + 2 : HEAD + 3, :] = end_row
     states_ref[x, HEAD + 3 :, :] = jnp.zeros((STATE_ROWS - HEAD - 3, width), jnp.float32)
 
     def state_sends():
         for step in range(1, across):
             yield remote(
-                states_ref.at[x], states_ref.at[x], st_send.at[step], st_recv.at[x], "sp",
+                states_ref.at[x], states_ref.at[x], st_send, st_recv.at[x], "sp",
                 z * across + lax.rem(x + step, across),
             )
 
@@ -391,31 +393,42 @@
         step_rows = 128
         for group in range(groups):
             lane_group = slice(group * 128, (group + 1) * 128)
+            heads_here = (2 * group, 2 * group + 1)
+            upper_half = lax.broadcasted_iota(jnp.int32, (128, step_rows), 0) < HEAD
             for start in range(0, rows, step_rows):
                 stop = start + step_rows
-                block_rows = slice(start, stop)
-                keys = mk_ref[:stop, lane_group]
-                values = mv_ref[:stop, lane_group]
-                group_queries = mq_ref[block_rows, lane_group]
-                row_index = lax.broadcasted_iota(jnp.int32, (step_rows, stop), 0)
-                column_index = lax.broadcasted_iota(jnp.int32, (step_rows, stop), 1)
-                lower = column_index <= row_index + start
-                result = None
-                for side in range(2):
-                    head = group * 2 + side
-                    chosen = (lanes // HEAD) == side
-                    column = cumulative_ref[block_rows, head : head + 1]
-                    gaps = jnp.where(lower, column + offset_ref[head : head + 1, :stop], NEGATIVE)
-                    row_top = jnp.max(gaps, axis=1, keepdims=True)
-                    within = jnp.exp(gaps - row_top)
-                    scores = dot(jnp.where(chosen, group_queries, 0), keys, ((1,), (1,)))
-                    scores = jnp.where(lower, within * (scores * (HEAD**-0.5)), 0.0)
-                    inner_den[block_rows, head : head + 1] = jnp.sum(scores, axis=1, keepdims=True)
-                    inner_top[block_rows, head : head + 1] = row_top
-                    score_high, score_low = two_parts(scores)
-                    numerator = dot(score_high, values) + dot(score_low, values)
-                    result = numerator if result is None else jnp.where(chosen, numerator, result)
-                inner_ref[block_rows, lane_group] = result
+                here = slice(start, stop)
+                queries = mq_turned[lane_group, here].astype(jnp.float32)
+                both = jnp.concatenate(
+                    [jnp.where(upper_half, queries, 0.0), jnp.where(upper_half, 0.0, queries)], axis=1
+                ).astype(jnp.bfloat16)
+                scores = dot(mk_ref[:stop, lane_group], both)
+                ahead = jnp.concatenate(
+                    [cumulative_ref[head : head + 1, here] for head in heads_here], axis=1
+                )
+                behind = jnp.concatenate(
+                    [
+                        jnp.broadcast_to(offset_ref[:stop, head : head + 1], (stop, step_rows))
+                        for head in heads_here
+                    ],
+                    axis=1,
+                )
+                key_index = lax.broadcasted_iota(jnp.int32, scores.shape, 0)
+                query_index = lax.broadcasted_iota(jnp.int32, scores.shape, 1) % step_rows
+                gaps = jnp.where(key_index <= query_index + start, ahead + behind, NEGATIVE)
+                row_top = jnp.max(gaps, axis=0, keepdims=True)
+                scores = jnp.exp(gaps - row_top) * (scores * (HEAD**-0.5))
+                total = jnp.sum(scores, axis=0, keepdims=True)
+                for side, head in enumerate(heads_here):
+                    lanes_at = slice(side * step_rows, (side + 1) * step_rows)
+                    inner_den[head : head + 1, here] = total[:, lanes_at]
+                    inner_top[head : head + 1, here] = row_top[:, lanes_at]
+                score_high, score_low = two_parts(scores)
+                values = mv_turned[lane_group, :stop]
+                numerator = dot(values, score_high) + dot(values, score_low)
+                inner_ref[lane_group, here] = jnp.where(
+                    upper_half, numerator[:, :step_rows], numerator[:, step_rows:]
+                )
 
     def advance(body, stable, later):
         later_top = later[HEAD + 1 : HEAD + 2, :]
@@ -450,7 +463,7 @@
         for step in range(1, across):
             other = lax.rem(x + step, across)
             at = states_ref.at[other]
-            remote(at, at, st_send.at[step], st_recv.at[other], "sp", me).wait_recv()
+            remote(at, at, st_send, st_recv.at[other], "sp", me).wait_recv()
 
         @pl.when(z == 0)
         def _():
@@ -506,9 +519,8 @@
     def arrive(origin):
         @pl.when((origin != me) & (lax.rem(origin, parts) != my_part))
         def _():
-            for chunk in range(chunks):
-                at = kv_all.at[origin, rows_of(chunk)]
-                remote(at, at, kv_send.at[0, chunk], kv_recv.at[origin, chunk], "sp", me).wait_recv()
+            at = kv_all.at[origin]
+            remote(at, at, fwd_send, cross_recv.at[origin], "sp", me).wait_recv()
 
         turned = kv_all[origin].T
         vt_ref[origin, :HEAD, :] = turned[HEAD:, :]
@@ -520,11 +532,8 @@
 
             @pl.when(origin != me)
             def _():
-                for chunk in range(chunks):
-                    at = q_all.at[slot, packed_of(chunk)]
-                    remote(
-                        at, at, q_send.at[0, chunk], q_recv.at[slot, chunk], "sp", me
-                    ).wait_recv()
+                at = q_all.at[slot]
+                remote(at, at, q_send, q_recv.at[slot], "sp", me).wait_recv()
 
             for chunk in range(chunks):
                 wave = chunk * span // half_rows
@@ -609,7 +618,7 @@
 
     def att_copy(slot, wave):
         return remote(
-            att_out.at[slot, wave], att_place(wave), att_send.at[slot, wave],
+            att_out.at[slot, wave], att_place(wave), att_send,
             att_recv.at[my_head, wave], "sp", span_of(slot),
         )
 
@@ -633,39 +642,43 @@
                 att_copy(slot, wave).start()
 
     def recall():
-        stable = enter_ref[HEAD + 1 : HEAD + 2, :]
         memory_in = enter_ref[:HEAD, :]
         normal_in = enter_ref[HEAD : HEAD + 1, :]
+        head_of_lane = lax.broadcasted_iota(jnp.int32, (16, width), 1) // HEAD
+        head_of_row = lax.broadcasted_iota(jnp.int32, (16, width), 0)
         blocks = jnp.concatenate(
-            [jnp.where(head_mask(width, head), memory_in, 0.0) for head in range(heads)], axis=0
+            [jnp.where(head_mask(width, head), memory_in, 0.0) for head in range(heads)]
+            + [jnp.where(head_of_lane == head_of_row, normal_in, 0.0)],
+            axis=0,
         )
         high, low = two_parts(blocks)
-        memory_queries = mq_ref[...]
-        carried_part = dot(memory_queries, high) + dot(memory_queries, low)
-        weighted = memory_queries.astype(jnp.float32) * normal_in
-        for group in range(groups):
-            lane_group = slice(group * 128, (group + 1) * 128)
-            result = None
-            for side in range(2):
-                head = group * 2 + side
-                chosen = (lanes // HEAD) == side
-                column = slice(head, head + 1)
-                carried_log = cumulative_ref[:, column] + stable[:, head * HEAD : head * HEAD + 1]
-                own_top = inner_top[:, column]
-                row_top = jnp.maximum(carried_log, own_top)
-                inside = jnp.exp(own_top - row_top)
-                outside = jnp.exp(carried_log - row_top)
-                denominator = inside * inner_den[:, column] + outside * jnp.sum(
-                    jnp.where(chosen, weighted[:, lane_group], 0.0), axis=1, keepdims=True
-                )
-                numerator = inside * inner_ref[:, lane_group] + outside * carried_part[:, lane_group]
-                quotient = numerator / jnp.maximum(jnp.abs(denominator), 1.0)
-                result = quotient if result is None else jnp.where(chosen, quotient, result)
-            memory_ref[:, lane_group] = result.astype(jnp.bfloat16)
-
+        carried = dot(high, mq_turned[...]) + dot(low, mq_turned[...])
+        head_rows = lax.broadcasted_iota(jnp.int32, (heads, 1), 0)
+        stable = jnp.zeros((heads, 1), jnp.float32)
+        for head in range(heads):
+            stable = jnp.where(
+                head_rows == head,
+                enter_ref[HEAD + 1 : HEAD + 2, head * HEAD : head * HEAD + 1],
+                stable,
+            )
+        carried_log = cumulative_ref[:heads] + stable
+        own_top = inner_top[:heads]
+        row_top = jnp.maximum(carried_log, own_top)
+        inside = jnp.exp(own_top - row_top)
+        outside = jnp.exp(carried_log - row_top)
+        denominator = inside * inner_den[:heads] + outside * carried[width : width + heads]
+        denominator = jnp.maximum(jnp.abs(denominator), 1.0)
+        inside = inside / denominator
+        outside = outside / denominator
+        for head in range(heads):
+            at = slice(head * HEAD, (head + 1) * HEAD)
+            one = slice(head, head + 1)
+            memory_ref[at, :] = (inside[one] * inner_ref[at, :] + outside[one] * carried[at]).astype(
+                jnp.bfloat16
+            )
         loads[6].wait()
         loads[7].wait()
-        partial_ref[...] = dot(memory_ref[...], som[...])
+        partial_ref[...] = dot(memory_ref[...], som[...], ((0,), (0,)))
 
     settle(me // 2)
     within(me // 2, (0, 1))
@@ -676,7 +689,6 @@
     lax.fori_loop(1, units - 1, visit, 0)
     last = visit_unit(units - 1)
     settle(last)
-    pl.when(z == units - 2)(chain)
     for wave in range(2):
         within(last, (wave,))
         if parts == 2:
@@ -696,6 +708,7 @@
             lax.fori_loop(0, units - 1, earlier, 0)
         finish(wave)
         if wave == 0:
+            pl.when(z == units - 2)(chain)
             pl.when(z < units - 1)(recall)
     @pl.when(z >= units - 1)
     def _():
@@ -724,7 +737,7 @@
             line_out[step, out_rows(chunk), :] = pair_sum(step, chunk).astype(jnp.bfloat16)
             copy = remote(
                 line_out.at[step, out_rows(chunk)], line_in.at[step, out_rows(chunk)],
-                sl_send.at[step, chunk], sl_recv.at[step, chunk], "tp",
+                sl_send, sl_recv.at[step - 1, chunk], "tp",
                 lax.rem(line + step, lines) * CORES + core,
             )
             copy.start()
@@ -736,7 +749,7 @@
             @pl.when((my_owner != my_part) | (my_head != step))
             def _():
                 at = attended_ref.at[wave, pl.ds(step * HEAD, HEAD)]
-                remote(at, at, att_send.at[0, wave], att_recv.at[step, wave], "sp", me).wait_recv()
+                remote(at, at, att_send, att_recv.at[step, wave], "sp", me).wait_recv()
 
         at = slice(wave * half_rows, (wave + 1) * half_rows)
         part_ref[at, :] = (
@@ -747,7 +760,7 @@
                 target = lax.rem(line + step, lines) * CORES + (1 - core)
                 copy = remote(
                     part_ref.at[out_rows(chunk), columns_of(target)],
-                    pair_in.at[step, out_rows(chunk)], sp_send.at[step, chunk],
+                    pair_in.at[step, out_rows(chunk)], sp_send,
                     sp_recv.at[step, chunk], "tp", pair,
                 )
                 copy.start()
@@ -755,43 +768,33 @@
         for chunk in range(wave * per_wave, (wave + 1) * per_wave):
             pass_on(chunk)
 
-    for copy in sends:
-        copy.wait_send()
-    for copy in pairs.values():
-        copy.wait_send()
-    for chunk in range(chunks):
-        for copy in kv_sends(chunk):
-            copy.wait_send()
-        for copy in q_sends(chunk):
-            copy.wait_send()
-        for index in range(heads):
-            for copy in forwards(kv_all.at[0, rows_of(chunk)], 0, index, chunk):
-                copy.wait_send()
-
-        @pl.when(my_owner != my_part)
-        def _():
-            q_aside(chunk).wait_send()
-
-    for copy in state_sends():
-        copy.wait_send()
+    def sent(ref, semaphore):
+        remote(ref, ref, semaphore, semaphore, "tp", pair).wait_send()
+
+    others = line_in.at[pl.ds(1, lines - 1)]
+    sent(others, line_send)
+    sent(pair_in, pair_send)
+    sent(kv_out.at[pl.ds(0, heads - 1)], kv_send)
+    sent(kv_all.at[pl.ds(0, heads * (parts - 1))], fwd_send)
+    sent(q_out.at[pl.ds(0, heads - 1)], q_send)
+    pl.when(my_owner != my_part)(lambda: sent(q_out.at[0], q_side))
+    sent(states_ref.at[pl.ds(0, across - 1)], st_send)
     pl.when(z < depth - 1)(lambda: prefix_send().wait_send())
-    for slot in range(heads):
-
-        @pl.when(span_of(slot) != me)
-        def _():
-            for wave in range(2):
-                att_copy(slot, wave).wait_send()
-
+    pl.when(my_owner == my_part)(lambda: sent(att_out.at[pl.ds(0, heads - 1)], att_send))
+    pl.when(my_owner != my_part)(lambda: sent(att_out, att_send))
     for chunk in range(out_chunks):
         total = pair_sum(0, chunk)
         for step in range(1, lines):
             lined[step, chunk].wait_recv()
             total = total + line_in[step, out_rows(chunk), :].astype(jnp.float32)
-        out_ref[out_rows(chunk), :] = total.astype(jnp.bfloat16)
-    for copy in swaps.values():
-        copy.wait_send()
-    for copy in lined.values():
-        copy.wait_send()
+        total_ref[out_rows(chunk), :] = total.astype(jnp.bfloat16)
+        copy = pltpu.make_async_copy(
+            total_ref.at[out_rows(chunk)], out_ref.at[out_rows(chunk)], out_sem
+        )
+        copy.start()
+    pltpu.make_async_copy(total_ref, out_ref, out_sem).wait()
+    sent(pair_in, sp_send)
+    sent(others, sl_send)
 
 
 def per_device(tp_size, depth, across, inputs, norm_gain, query_weight, key_weight, value_weight,
@@ -809,8 +812,6 @@
     out_chunks = 4
     dma = pltpu.SemaphoreType.DMA
 
-    middle = DD // 2
-    inverse = 1.0 / ROTARY_BASE ** (jnp.arange(middle, dtype=jnp.float32) / middle)
 
     hbm = pl.BlockSpec(memory_space=pl.ANY)
     bf16 = lambda *shape: pltpu.VMEM(shape, jnp.bfloat16)
@@ -818,8 +819,8 @@
     return pl.pallas_call(
         functools.partial(layer_kernel, tp_size, depth, across, chunks, out_chunks),
         out_shape=jax.ShapeDtypeStruct((rows, columns), jnp.bfloat16),
-        in_specs=[VMEM] * 3 + [hbm] * 6 + [VMEM] * 6 + [hbm] * 2,
-        out_specs=VMEM,
+        in_specs=[VMEM] * 2 + [hbm] * 6 + [VMEM] * 6 + [hbm] * 2,
+        out_specs=hbm,
         scratch_shapes=[bf16(features, 6 * width)]
         + [bf16(width, features)] * 2
         + [
@@ -830,28 +831,28 @@
             bf16(2, rows, 128), bf16(heads, 2, 128, rows), f32(heads, 2, 1, rows),
             f32(heads, 2, VALUE_ROWS, rows), bf16(heads, 2, HEAD, rows // 2),
             bf16(2, width, rows // 2),
-            bf16(rows, width), bf16(rows, width), bf16(rows, width), f32(rows, 128),
+            bf16(rows, width), bf16(rows, width), bf16(rows, width), bf16(width, rows),
+            bf16(width, rows), f32(rows, 128),
             f32(across, STATE_ROWS, width), f32(STATE_ROWS, width), f32(STATE_ROWS, width),
             f32(STATE_ROWS, width),
-            f32(rows, width), f32(rows, 128), f32(rows, 128), f32(rows, 128), f32(8, rows),
-            bf16(rows, width),
+            f32(width, rows), f32(8, rows), f32(8, rows), f32(8, rows), f32(rows, 128),
+            bf16(width, rows),
             f32(rows, features), bf16(rows, features), bf16(lines, rows, columns),
             bf16(lines, rows, columns),
-            bf16(lines, rows, columns),
-            dma((8,)), dma((lines, chunks)), dma((lines, chunks)), dma((lines, chunks)),
-            dma((lines, chunks)),
-            dma((heads, chunks)), dma((heads, parts, chunks)), dma((spans, chunks)),
-            dma((heads, chunks)), dma((heads, chunks)), dma((heads, 2)), dma((heads, 2)),
-            dma((across,)), dma((across,)), dma(()), dma(()),
-            dma((lines, out_chunks)), dma((lines, out_chunks)), dma((lines, out_chunks)),
-            dma((lines, out_chunks)),
+            bf16(lines, rows, columns), bf16(rows, columns),
+            dma(()), dma((8,)), dma(()), dma((lines - 1, chunks)), dma(()),
+            dma((lines - 1, chunks)), dma(()),
+            dma(()), dma(()), dma((heads, chunks)), dma((spans,)), dma(()), dma(()),
+            dma((heads,)), dma(()), dma((heads, 2)),
+            dma(()), dma((across,)), dma(()), dma(()), dma(()), dma((lines, out_chunks)), dma(()),
+            dma((lines - 1, out_chunks)),
         ],
         compiler_params=pltpu.CompilerParams(
             vmem_limit_bytes=VMEM_LIMIT, collective_id=0, has_side_effects=True
         ),
         name="layer",
     )(
-        inputs, norm_gain[None, :], inverse[:, None], query_weight, key_weight, value_weight,
+        inputs, norm_gain[None, :], query_weight, key_weight, value_weight,
         memory_query_weight, memory_key_weight, memory_value_weight, input_gate_weight.T,
         forget_gate_weight.T, forget_bias[None, :], decay_shift.T, lambdas[None, :],
         head_gain[None, :], out_weight_attention, out_weight_memory,

time: 56.4 us -> 53 us (0.940)
  Pallas kernels: 53.9 us -> 51 us
  other arithmetic: 0.61 us -> 0 us
    pallas_call x1, Pallas kernels: 53.9 us -> 51 us  [per_device(): pl.pallas_call(functools.partial(layer_kernel, tp_size, depth, across, ch...]
    pow x1 -> x0, other arithmetic: 0.61 us -> none  [per_device(): ROTARY_BASE ** (jnp.arange(middle, dtype=jnp.float32) / middle)]
where the time goes in v4:
time: 53 us; the launch traced here: 52.8 us
  Pallas kernels  51 us (96%)
  local copies, waits for them, and re-layouts  1.77 us (3%)
    pallas_call x1, Pallas kernels, per_device(): pl.pallas_call(functools.partial(layer_kernel, tp_size, depth, across, ch...  51 us
    unnamed x1, local copies, waits for them, and re-layouts  1.77 us

profile of v4, /device:TPU:0, one launch (start us, length us, event | category | flops | bytes accessed | tf_op | source)
XLA Modules:
  0.0 52.8 jit_solution(10147270997036009496)
XLA Ops:
  0.0 51.0 %layer.1 = bf16[384,512]{1,0:T(8,128)(2,1)} custom-call(bf16[384,512]{1,0:T(8,128)(2,1)} %shard_ref.1, f32[1,2048]{1,0:T(1,128)} %bitcast.9, bf16[2048,256]{1,0:T(8,128)(2,1)} %wq.1, bf16[2048,256]{1,0:T(8,128)(2,1)} %wk.1, bf16[2048,256]{1,0:T(8,128)(2,1)} %wv.1, bf16[2048,256]{1,0:T(8,128)(2,1)} %wmq.1, bf16[2048,256]{1,0:T(8,128)(2,1)} %wmk.1, ...), custom_call_target="tpu_custom_call" | custom-call | tf_op jit(solution)/shard_map/layer/pallas_call | solution.py:819
  51.0 1.8 %copy.18 = bf16[384,512]{1,0:T(8,128)(2,1)} copy(bf16[384,512]{1,0:T(8,128)(2,1)} %layer.1) | data formatting | bytes 786432

commit v5 on v4

--- a/solution.py
+++ b/solution.py
@@ -67,7 +67,8 @@
     out_ref,
     weight_ref, soa, som, x_ref, scaled_ref, square_ref, sum_ref, cosine_ref, sine_ref,
     kv_out, q_out, kv_all, q_all, vt_ref, qn_ref, qt_ref, top_ref, acc_ref, att_out, attended_ref,
-    mq_ref, mk_ref, mv_ref, mq_turned, mv_turned, pre_ref, states_ref, prefix_in, prefix_out, enter_ref,
+    mq_ref, mk_ref, mv_ref, mq_turned, mv_turned, pre_ref, states_ref, state_rows, prefix_in, row_in, prefix_out, row_out,
+    enter_ref,
     inner_ref, inner_den, inner_top, cumulative_ref, offset_ref, memory_ref,
     partial_ref, part_ref, pair_in, line_out, line_in, total_ref,
     out_sem, load_sems, line_send, line_recv, pair_send, pair_recv, own_recv,
@@ -372,18 +373,18 @@
         normal = jnp.where(chosen, whole[width + head : width + head + 1, :], normal)
         top_row = jnp.where(chosen, top[at_head], top_row)
         end_row = jnp.where(chosen, end[at_head], end_row)
-    states_ref[x, :HEAD, :] = memory
-    states_ref[x, HEAD : HEAD + 1, :] = normal
-    states_ref[x, HEAD + 1 : HEAD + 2, :] = top_row
-    states_ref[x, HEAD + 2 : HEAD + 3, :] = end_row
-    states_ref[x, HEAD + 3 :, :] = jnp.zeros((STATE_ROWS - HEAD - 3, width), jnp.float32)
+    states_ref[x] = memory.astype(jnp.bfloat16)
+    state_rows[x] = jnp.concatenate(
+        [normal, top_row, end_row, jnp.zeros((5, width), jnp.float32)], axis=0
+    )
 
     def state_sends():
         for step in range(1, across):
-            yield remote(
-                states_ref.at[x], states_ref.at[x], st_send, st_recv.at[x], "sp",
-                z * across + lax.rem(x + step, across),
-            )
+            for index, ref in enumerate((states_ref, state_rows)):
+                yield remote(
+                    ref.at[x], ref.at[x], st_send.at[index], st_recv.at[index, x], "sp",
+                    z * across + lax.rem(x + step, across),
+                )
 
     forward("state")
     for copy in state_sends():
@@ -430,48 +431,65 @@
                     upper_half, numerator[:, :step_rows], numerator[:, step_rows:]
                 )
 
-    def advance(body, stable, later):
-        later_top = later[HEAD + 1 : HEAD + 2, :]
-        decay = later[HEAD + 2 : HEAD + 3, :]
+    def advance(memory, normal, stable, other):
+        later_top = state_rows[other, 1:2, :]
+        decay = state_rows[other, 2:3, :]
         new = jnp.maximum(decay + stable, later_top)
-        return jnp.exp(decay + stable - new) * body + jnp.exp(later_top - new) * later, new
-
-    def prefix_send():
-        return remote(
-            prefix_out, prefix_in, px_send, px_recv, "sp", jnp.minimum(me + across, spans - 1)
+        former = jnp.exp(decay + stable - new)
+        latter = jnp.exp(later_top - new)
+        return (
+            former * memory + latter * states_ref[other].astype(jnp.float32),
+            former * normal + latter * state_rows[other, 0:1, :],
+            new,
         )
 
-    def level(body, stable):
-        for other in range(across):
-
-            @pl.when(x == other)
-            def _():
-                enter_ref[...] = body
-                enter_ref[HEAD + 1 : HEAD + 2, :] = stable
-
-            if other < across - 1:
-                body, stable = advance(body, stable, states_ref[other])
-        body, stable = advance(body, stable, states_ref[across - 1])
-
-        @pl.when(z < depth - 1)
-        def _():
-            prefix_out[...] = body
-            prefix_out[HEAD + 1 : HEAD + 2, :] = stable
-            prefix_send().start()
+    prefixes = ((prefix_out, prefix_in), (row_out, row_in))
+
+    def prefix_sends():
+        for index, (source, target) in enumerate(prefixes):
+            yield remote(
+                source, target, px_send.at[index], px_recv.at[index], "sp",
+                jnp.minimum(me + across, spans - 1),
+            )
 
     def chain():
         for step in range(1, across):
             other = lax.rem(x + step, across)
-            at = states_ref.at[other]
-            remote(at, at, st_send, st_recv.at[other], "sp", me).wait_recv()
+            for index, ref in enumerate((states_ref, state_rows)):
+                at = ref.at[other]
+                remote(
+                    at, at, st_send.at[index], st_recv.at[index, other], "sp", me
+                ).wait_recv()
 
         @pl.when(z == 0)
         def _():
-            prefix_in[...] = jnp.zeros((STATE_ROWS, width), jnp.float32)
-
-        pl.when(z > 0)(lambda: prefix_send().wait_recv())
-        body = prefix_in[...]
-        level(body, body[HEAD + 1 : HEAD + 2, :])
+            prefix_in[...] = jnp.zeros((HEAD, width), jnp.bfloat16)
+            row_in[...] = jnp.zeros((8, width), jnp.float32)
+
+        @pl.when(z > 0)
+        def _():
+            for copy in prefix_sends():
+                copy.wait_recv()
+
+        carry = (prefix_in[...].astype(jnp.float32), row_in[0:1, :], row_in[1:2, :])
+        for other in range(across):
+
+            @pl.when(x == other)
+            def _():
+                enter_ref[:HEAD, :] = carry[0]
+                enter_ref[HEAD : HEAD + 1, :] = carry[1]
+                enter_ref[HEAD + 1 : HEAD + 2, :] = carry[2]
+
+            carry = advance(*carry, other)
+
+        @pl.when(z < depth - 1)
+        def _():
+            prefix_out[...] = carry[0].astype(jnp.bfloat16)
+            row_out[0:1, :] = carry[1]
+            row_out[1:2, :] = carry[2]
+            row_out[2:8, :] = jnp.zeros((6, width), jnp.float32)
+            for copy in prefix_sends():
+                copy.start()
 
     top_ref[...] = jnp.full(top_ref.shape, NEGATIVE, jnp.float32)
     acc_ref[...] = jnp.zeros(acc_ref.shape, jnp.float32)
@@ -778,8 +796,14 @@
     sent(kv_all.at[pl.ds(0, heads * (parts - 1))], fwd_send)
     sent(q_out.at[pl.ds(0, heads - 1)], q_send)
     pl.when(my_owner != my_part)(lambda: sent(q_out.at[0], q_side))
-    sent(states_ref.at[pl.ds(0, across - 1)], st_send)
-    pl.when(z < depth - 1)(lambda: prefix_send().wait_send())
+    sent(states_ref.at[pl.ds(0, across - 1)], st_send.at[0])
+    sent(state_rows.at[pl.ds(0, across - 1)], st_send.at[1])
+
+    @pl.when(z < depth - 1)
+    def _():
+        for copy in prefix_sends():
+            copy.wait_send()
+
     pl.when(my_owner == my_part)(lambda: sent(att_out.at[pl.ds(0, heads - 1)], att_send))
     pl.when(my_owner != my_part)(lambda: sent(att_out, att_send))
     for chunk in range(out_chunks):
@@ -833,8 +857,8 @@
             bf16(2, width, rows // 2),
             bf16(rows, width), bf16(rows, width), bf16(rows, width), bf16(width, rows),
             bf16(width, rows), f32(rows, 128),
-            f32(across, STATE_ROWS, width), f32(STATE_ROWS, width), f32(STATE_ROWS, width),
-            f32(STATE_ROWS, width),
+            bf16(across, HEAD, width), f32(across, 8, width), bf16(HEAD, width), f32(8, width),
+            bf16(HEAD, width), f32(8, width), f32(STATE_ROWS, width),
             f32(width, rows), f32(8, rows), f32(8, rows), f32(8, rows), f32(rows, 128),
             bf16(width, rows),
             f32(rows, features), bf16(rows, features), bf16(lines, rows, columns),
@@ -844,7 +868,8 @@
             dma((lines - 1, chunks)), dma(()),
             dma(()), dma(()), dma((heads, chunks)), dma((spans,)), dma(()), dma(()),
             dma((heads,)), dma(()), dma((heads, 2)),
-            dma(()), dma((across,)), dma(()), dma(()), dma(()), dma((lines, out_chunks)), dma(()),
+            dma((2,)), dma((2, across)), dma((2,)), dma((2,)), dma(()), dma((lines, out_chunks)),
+            dma(()),
             dma((lines - 1, out_chunks)),
         ],
         compiler_params=pltpu.CompilerParams(

time: 53 us -> 52.7 us (level)
  no operation moved by 1% of the time
where the time goes in v5:
time: 52.7 us; the launch traced here: 52.5 us
  Pallas kernels  50.7 us (96%)
  local copies, waits for them, and re-layouts  1.77 us (3%)
    pallas_call x1, Pallas kernels, per_device(): pl.pallas_call(functools.partial(layer_kernel, tp_size, depth, across, ch...  50.7 us
    unnamed x1, local copies, waits for them, and re-layouts  1.77 us

profile of v5, /device:TPU:0, one launch (start us, length us, event | category | flops | bytes accessed | tf_op | source)
XLA Modules:
  0.0 52.5 jit_solution(15727499597096349358)
XLA Ops:
  0.0 50.7 %layer.1 = bf16[384,512]{1,0:T(8,128)(2,1)} custom-call(bf16[384,512]{1,0:T(8,128)(2,1)} %shard_ref.1, f32[1,2048]{1,0:T(1,128)} %bitcast.9, bf16[2048,256]{1,0:T(8,128)(2,1)} %wq.1, bf16[2048,256]{1,0:T(8,128)(2,1)} %wk.1, bf16[2048,256]{1,0:T(8,128)(2,1)} %wv.1, bf16[2048,256]{1,0:T(8,128)(2,1)} %wmq.1, bf16[2048,256]{1,0:T(8,128)(2,1)} %wmk.1, ...), custom_call_target="tpu_custom_call" | custom-call | tf_op jit(solution)/shard_map/layer/pallas_call | solution.py:843
  50.7 1.8 %copy.18 = bf16[384,512]{1,0:T(8,128)(2,1)} copy(bf16[384,512]{1,0:T(8,128)(2,1)} %layer.1) | data formatting | bytes 786432

commit v6 on v5

--- a/solution.py
+++ b/solution.py
@@ -640,8 +640,8 @@
             att_recv.at[my_head, wave], "sp", span_of(slot),
         )
 
-    def finish(wave):
-        for slot in range(heads):
+    def finish(wave, slots):
+        for slot in slots:
             sums = acc_ref[slot, wave]
             maps = sums[:HEAD] / sums[HEAD : HEAD + 1]
             second = pltpu.roll(maps, half_rows, 1)[:, :half_rows]
@@ -707,8 +707,11 @@
     lax.fori_loop(1, units - 1, visit, 0)
     last = visit_unit(units - 1)
     settle(last)
+    pl.when(z == units - 2)(chain)
+    within(last, (0, 1))
     for wave in range(2):
-        within(last, (wave,))
+        finish(wave, (0,))
+    for wave in range(2):
         if parts == 2:
             steps = []
             for rank in range(units - 1):
@@ -724,14 +727,10 @@
                 return unused
 
             lax.fori_loop(0, units - 1, earlier, 0)
-        finish(wave)
+        finish(wave, range(1, heads))
         if wave == 0:
-            pl.when(z == units - 2)(chain)
-            pl.when(z < units - 1)(recall)
-    @pl.when(z >= units - 1)
-    def _():
-        chain()
-        recall()
+            pl.when(z == units - 1)(chain)
+            recall()
 
     out_span = rows // out_chunks
     per_wave = out_chunks // 2

time: 52.7 us -> 54.2 us (1.028)
  the two profiles are of different devices: /device:TPU:0 before, /device:TPU:9 now
where the time goes in v6:
time: 54.2 us; the launch traced here: 54 us
  Pallas kernels  52.3 us (96%)
  local copies, waits for them, and re-layouts  1.77 us (3%)
    pallas_call x1, Pallas kernels, per_device(): pl.pallas_call(functools.partial(layer_kernel, tp_size, depth, across, ch...  52.3 us
    unnamed x1, local copies, waits for them, and re-layouts  1.77 us

profile of v6, /device:TPU:9, one launch (start us, length us, event | category | flops | bytes accessed | tf_op | source)
XLA Modules:
  0.0 54.0 jit_solution(4513719856972807079)
XLA Ops:
  0.0 52.3 %layer.1 = bf16[384,512]{1,0:T(8,128)(2,1)} custom-call(bf16[384,512]{1,0:T(8,128)(2,1)} %shard_ref.1, f32[1,2048]{1,0:T(1,128)} %bitcast.9, bf16[2048,256]{1,0:T(8,128)(2,1)} %wq.1, bf16[2048,256]{1,0:T(8,128)(2,1)} %wk.1, bf16[2048,256]{1,0:T(8,128)(2,1)} %wv.1, bf16[2048,256]{1,0:T(8,128)(2,1)} %wmq.1, bf16[2048,256]{1,0:T(8,128)(2,1)} %wmk.1, ...), custom_call_target="tpu_custom_call" | custom-call | tf_op jit(solution)/shard_map/layer/pallas_call | solution.py:842
  52.3 1.8 %copy.18 = bf16[384,512]{1,0:T(8,128)(2,1)} copy(bf16[384,512]{1,0:T(8,128)(2,1)} %layer.1) | data formatting | bytes 786432
